TPU v7x, 512 devices: a whole 4x8x8 slice. The times are simulated.
512 devices in a mesh: dp: 4 (over x), kv: 64 (over z, y), tp: 2 (over core).
Axes of the slice: x: 4, y: 8, z: 8, core: 2. Of those that a mesh axis runs over, the one named last changes fastest.
Arguments:
- tokens: bfloat16 [512, 4, 4096], P('dp', None, 'kv'), may hold values from -260 to 260
- norm_gain: bfloat16 [4096], replicated, may hold values from 0.099609375 to 1.8984375
- query_weight: bfloat16 [4096, 2048], P(None, ('tp', 'kv')), may hold values from -0.09375 to 0.09375
- key_weight: bfloat16 [4096, 2048], P(None, ('tp', 'kv')), may hold values from -0.09375 to 0.09375
- value_weight: bfloat16 [4096, 4096], P(None, ('tp', 'kv')), may hold values from -0.09375 to 0.09375
- gate_weight: bfloat16 [4096, 4096], P(None, ('tp', 'kv')), may hold values from -0.09375 to 0.09375
- out_weight: bfloat16 [4096, 4096], P('tp', 'kv'), may hold values from -0.09375 to 0.09375
- decay_rate: float32 [16], P('tp'), may hold values from 0.02 to 1
- prior_state: float32 [512, 16, 128, 256], P(('dp', 'kv'), 'tp'), may hold values from -0.6 to 0.6
- last_keys: bfloat16 [512, 4, 16, 128], P(('dp', 'kv'), None, 'tp'), may hold values from -0.5390625 to 0.5390625
- last_values: bfloat16 [512, 4, 16, 256], P(('dp', 'kv'), None, 'tp'), may hold values from -6 to 6
- accepted: int32 [512], P(('dp', 'kv')), may hold values from 0 to 4
- lengths: int32 [512], P(('dp', 'kv')), may hold values from 16 to 99999
Outputs:
- retained: bfloat16 [512, 4, 4096], P('dp', None, ('kv', 'tp'))
- new_state: float32 [512, 16, 128, 256], P(('dp', 'kv'), 'tp')
- new_keys: bfloat16 [512, 4, 16, 128], P(('dp', 'kv'), None, 'tp')
- new_values: bfloat16 [512, 4, 16, 256], P(('dp', 'kv'), None, 'tp')
Inputs may be any that keep to these rules, and one draw needn't show every extreme that they name: `accepted`: how many of the last step's 4 proposals were taken.
All inputs are finite; a program needn't handle non-finite values.
Results may differ from a plain program's by a relative error of at most 0.012.
Values may be sent and summed in bfloat16 or wider, within the bound.
A program may use at most 64 MiB of HBM per device.

v0:
```python
import jax
import jax.numpy as jnp
from jax import lax
from jax.sharding import Mesh
from jax.sharding import PartitionSpec as P

KV = ("kv_0", "kv_1")
TP_KV = ("tp", "kv_0", "kv_1")
DP_KV = ("dp", "kv_0", "kv_1")
KV_TP = ("kv_0", "kv_1", "tp")


epsilon = 1e-06


def over_axes(value, axes):
    for axis in axes:
        value = lax.psum(value, axis)
    return value


def swapped(value, axis, bit):
    return lax.ppermute(value, axis, [(i, i ^ 1 << bit) for i in range(lax.axis_size(axis))])


def laid_out(blocks, dim):
    lengths = list(blocks.shape[1:])
    lengths[dim] *= blocks.shape[0]
    return jnp.moveaxis(blocks, 0, dim).reshape(lengths)


def stacked_from(value, axes, turns):
    blocks = value[None]
    for k in turns:
        blocks = lax.all_gather(blocks, axes[k], axis=0, tiled=True)
    carried = [lax.axis_size(axes[k]) for k in reversed(turns)]
    blocks = blocks.reshape(*carried, *value.shape)
    turned = sorted(range(len(turns)), key=lambda place: turns[len(turns) - 1 - place])
    return blocks.transpose(*turned, *range(len(turns), blocks.ndim)).reshape(-1, *value.shape)


def gathered_by_axis(value, axes, turns, dim):
    return laid_out(stacked_from(value, axes, turns), dim)


def in_blocks(value, dim, length):
    before, after = (value.shape[:dim], value.shape[dim + 1 :])
    return jnp.moveaxis(value.reshape(*before, length, -1, *after), dim, 0)


def summed_on_arrival(value, axis, dim):
    length = lax.axis_size(axis)
    blocks = lax.all_to_all(in_blocks(value, dim, length), axis, 0, 0, tiled=True)
    return jnp.sum(blocks.astype(jnp.float32), axis=0)


def rotate(field_in, positions):
    half_size = field_in.shape[-1] // 2
    frequency = jnp.power(10000.0, -jnp.arange(half_size, dtype=jnp.float32) / half_size)
    angles = positions.astype(jnp.float32)[:, :, None, None] * frequency
    cosine, sine_part = (jnp.cos(angles), jnp.sin(angles))
    floats = field_in.astype(jnp.float32)
    first_half, second = (floats[..., :half_size], floats[..., half_size:])
    return jnp.concatenate(
        [first_half * cosine - second * sine_part, first_half * sine_part + second * cosine],
        axis=-1,
    )


def retain(
    query_rot, key_rot, value_rows, prior_state, last_keys, last_values, accepted, log_decay
):
    highest = lax.Precision.HIGHEST
    proposals = query_rot.shape[1]
    step_ids = jnp.arange(proposals, dtype=jnp.int32)
    taken_mask = step_ids[None, :] < accepted[:, None]
    power_exp = jnp.maximum(accepted[:, None] - 1 - step_ids[None, :], 0).astype(jnp.float32)
    weight = jnp.where(
        taken_mask[:, :, None], jnp.exp(log_decay[None, None, :] * power_exp[:, :, None]), 0.0
    )
    carried = jnp.exp(log_decay[None, :] * accepted[:, None].astype(jnp.float32))
    weighted_keys = last_keys.astype(jnp.float32) * weight[..., None]
    taken_state = carried[:, :, None, None] * prior_state + jnp.einsum(
        "sphd,sphe->shde", weighted_keys, last_values.astype(jnp.float32), precision=highest
    )
    scores = jnp.einsum(
        "sthd,smhd->shtm",
        query_rot.astype(jnp.float32),
        key_rot.astype(jnp.float32),
        precision=highest,
    )
    offset = (step_ids[:, None] - step_ids[None, :]).astype(jnp.float32)
    decay_grid = jnp.where(
        offset[None] >= 0.0, jnp.exp(log_decay[:, None, None] * jnp.maximum(offset, 0.0)[None]), 0.0
    )
    inner_sum = jnp.einsum(
        "shtm,smhe->sthe",
        scores * decay_grid[None],
        value_rows.astype(jnp.float32),
        precision=highest,
    )
    query_decay = jnp.exp(log_decay[None, :] * (step_ids[:, None].astype(jnp.float32) + 1.0))
    cross_sum = jnp.einsum(
        "sthd,shde->sthe",
        query_rot.astype(jnp.float32) * query_decay[None, :, :, None],
        taken_state,
        precision=highest,
    )
    return (inner_sum + cross_sum, taken_state)


def row_scale(tokens, row_block, first_row):
    partial_sq = jnp.sum(jnp.square(tokens.astype(jnp.float32)), axis=-1)
    total_sq = over_axes(partial_sq, KV)
    picked = lax.dynamic_slice_in_dim(total_sq, first_row, row_block.shape[1], 1)
    return lax.rsqrt(picked / row_block.shape[-1] + epsilon)


def shards(
    tokens,
    norm_gain,
    query_weight,
    key_weight,
    value_weight,
    gate_weight,
    out_weight,
    decay_rate,
    prior_state,
    last_keys,
    last_values,
    accepted,
    lengths,
):
    groups = lax.axis_size(KV)
    owned_seqs, proposals, _ = tokens.shape
    local_seqs, heads_here, key_size, value_size = prior_state.shape
    width = norm_gain.shape[0]
    key_cols = query_weight.shape[1]
    value_cols = value_weight.shape[1]
    col_span = 2 * key_cols + 2 * value_cols
    gain_vector = norm_gain.astype(jnp.float32)
    pair_index = lax.axis_index("tp")
    half_props = proposals // 2
    own_half = lax.dynamic_slice_in_dim(tokens, pair_index * half_props, half_props, 1)
    gathered = lax.all_gather(own_half, KV, axis=2, tiled=True)
    row_total = gathered.shape[0] * gathered.shape[1]
    scaled = (
        gathered.astype(jnp.float32)
        * row_scale(tokens, gathered, pair_index * half_props)[..., None]
        * gain_vector
    )
    normed = scaled.astype(jnp.bfloat16).reshape(row_total, width)
    own_weights = jnp.concatenate([query_weight, key_weight, value_weight, gate_weight], axis=1)
    other_weights = swapped(own_weights, "tp", 0)
    both_weights = jnp.where(
        pair_index == 0,
        jnp.concatenate([own_weights, other_weights], axis=1),
        jnp.concatenate([other_weights, own_weights], axis=1),
    )
    columns = jnp.dot(normed, both_weights, preferred_element_type=jnp.float32).astype(jnp.bfloat16)
    columns = columns.reshape(owned_seqs, half_props, 2 * col_span)
    arrived = lax.all_to_all(columns, KV, split_axis=0, concat_axis=2, tiled=True)
    arrived = arrived.reshape(local_seqs, half_props, groups, 2 * col_span)
    lower_part = arrived[..., :col_span]
    upper_part = arrived[..., col_span:]
    kept_part = jnp.where(pair_index == 0, lower_part, upper_part)
    sent_part = jnp.where(pair_index == 0, upper_part, lower_part)
    received = swapped(sent_part, "tp", 0)
    assembled = jnp.where(
        pair_index == 0,
        jnp.concatenate([kept_part, received], axis=1),
        jnp.concatenate([received, kept_part], axis=1),
    )

    def role_rows(first_col, col_count, last_size):
        picked = assembled[..., first_col : first_col + col_count]
        return picked.reshape(local_seqs, proposals, heads_here, last_size)

    query_rows = role_rows(0, key_cols, key_size)
    key_rows = role_rows(key_cols, key_cols, key_size)
    value_rows = role_rows(2 * key_cols, value_cols, value_size)
    gate_rows = role_rows(2 * key_cols + value_cols, value_cols, value_size)
    positions = (lengths + accepted)[:, None] + jnp.arange(proposals, dtype=jnp.int32)[None, :]
    query_rot = rotate(query_rows, positions).astype(jnp.bfloat16)
    key_rot = (rotate(key_rows, positions) * key_size ** (-0.5)).astype(jnp.bfloat16)
    heads_out, taken_state = retain(
        query_rot, key_rot, value_rows, prior_state, last_keys, last_values, accepted, -decay_rate
    )
    head_norm = heads_out * lax.rsqrt(
        jnp.mean(heads_out * heads_out, axis=-1, keepdims=True) + epsilon
    )
    gated = (jax.nn.silu(gate_rows.astype(jnp.float32)) * head_norm).astype(jnp.bfloat16)
    gated = gated.reshape(local_seqs, proposals, heads_here * value_size)
    gathered_piece = gathered_by_axis(gated, KV, (0, 1), 0)
    piece_rows = gathered_piece.shape[0]
    flat_rows = gathered_piece.reshape(piece_rows * proposals, heads_here * value_size)
    product = jnp.dot(flat_rows, out_weight, preferred_element_type=jnp.float32)
    partial_terms = product.reshape(piece_rows, proposals, out_weight.shape[1])
    retained = summed_on_arrival(partial_terms.astype(jnp.bfloat16), "tp", 2).astype(jnp.bfloat16)
    return (retained, taken_state, key_rot, value_rows)


def solution(mesh):
    finer = Mesh(
        mesh.devices.reshape(mesh.shape["dp"], 8, 8, mesh.shape["tp"]), ("dp", "kv_0", "kv_1", "tp")
    )
    return jax.shard_map(
        shards,
        mesh=finer,
        in_specs=(
            P("dp", None, KV),
            P(),
            P(None, TP_KV),
            P(None, TP_KV),
            P(None, TP_KV),
            P(None, TP_KV),
            P("tp", KV),
            P("tp"),
            P(DP_KV, "tp", None, None),
            P(DP_KV, None, "tp", None),
            P(DP_KV, None, "tp", None),
            P(DP_KV),
            P(DP_KV),
        ),
        out_specs=(
            P("dp", None, KV_TP),
            P(DP_KV, "tp", None, None),
            P(DP_KV, None, "tp", None),
            P(DP_KV, None, "tp", None),
        ),
        check_vma=False,
    )
```

profile of v0, /device:TPU:1, one launch (start us, length us, event | category | flops | bytes accessed | tf_op | source)
XLA Modules:
  0.0 229.2 jit_solution(18437961642913602430)
XLA Ops:
  7.2 0.0 copy-start
  7.2 0.0 copy-start.4
  7.3 0.0 all-gather.3.cloned.1.call-start
  7.3 1.6 constant_dynamic-slice_fusion
  8.9 0.0 all-gather.3.cloned.1.call-update
  8.9 2.0 pad_maximum_fusion
  11.0 8.7 %collective-permute-start = (bf16[4096,96]{0,1:T(8,128)(2,1)}, bf16[4096,96]{0,1:T(8,128)(2,1)}, u32[]{:S(2)}, u32[]{:S(2)}) collective-permute-start(bf16[4096,96]{0,1:T(8,128)(2,1)} %pad_maximum_fusion), channel_id=1, source_target_pairs={{0,1},{1,0},{2,3},{3,2},{4,5},{5,4},{6,7},{7,6},{8,9},{9,8},{10,11... | collective-permute-start | bytes 2359304 | tf_op jit(solution)/shard_map/ppermute | solution.py:23
  19.8 0.7 constant_dynamic-update-slice_fusion.4
  20.5 0.1 iota_compare_fusion
  20.6 0.1 maximum_convert_fusion
  20.6 0.1 multiply_exponential_fusion.1
  20.7 0.1 exponential_select_fusion
  20.8 0.1 exponential_select_fusion.1
  20.9 0.1 convert_multiply_fusion
  21.0 14.1 %psum.14 = f32[128,4]{0,1:T(4,128)S(1)} all-reduce(f32[128,4]{0,1:T(4,128)S(1)} %multiply_reduce_fusion), channel_id=1, replica_groups=mesh['dp'=4,'kv_0'=8,'kv_1'=8,'tp'=2] {'kv_0'}, use_global_device_ids=true, to_apply=%region_1.0 | all-reduce | flops 512 | bytes 4096 | tf_op jit(solution)/shard_map/psum | solution.py:18
  35.1 15.0 %psum.15 = f32[128,4]{0,1:T(4,128)S(1)} all-reduce(f32[128,4]{0,1:T(4,128)S(1)} %psum.14), channel_id=1, replica_groups=mesh['dp'=4,'kv_0'=8,'kv_1'=8,'tp'=2] {'kv_1'}, use_global_device_ids=true, to_apply=%region_2.0 | all-reduce | flops 512 | bytes 4096 | tf_op jit(solution)/shard_map/psum | solution.py:18
  50.1 0.7 constant_dynamic-update-slice_fusion.3
  50.8 0.7 constant_dynamic-update-slice_fusion.2
  51.5 2.8 %multiply_add_fusion = f32[2,8,128,256]{3,2,1,0:T(8,128)S(1)} fusion(f32[2,8,128,256]{3,2,1,0:T(8,128)} %param.21, f32[2,8]{1,0:T(2,128)S(1)} %multiply_exponential_fusion.1, bf16[2,4,8,256]{3,2,1,0:T(8,128)(2,1)S(1)} %copy-done.8, f32[2,4,8,128]{3,2,1,0:T(8,128)S(1)} %convert_multiply_fusion), kind=kOutput, calls=%fused_computation.2 | convolution fusion | flops 26214400 | bytes 4259904 | tf_op jit(solution)/shard_map/sphd,sphe->shde/dot_general | solution.py:83
  54.4 0.0 copy-start.1
  54.4 0.8 constant_dynamic-update-slice_fusion.1
  55.2 2.5 %constant_dynamic-update-slice_fusion.9 = (bf16[4096,192]{0,1:T(8,128)(2,1)}, bf16[4096,192]{0,1:T(8,128)(2,1)}) fusion(bf16[4096,96]{0,1:T(8,128)(2,1)} %collective-permute-done, bf16[4096,192]{0,1:T(8,128)(2,1)} %constant_dynamic-update-slice_fusion.1), kind=kLoop, calls=%fused_computation.49 | loop fusion | bytes 2359296
  57.7 0.7 constant_dynamic-update-slice_fusion.8
  58.3 0.7 constant_dynamic-update-slice_fusion.7
  59.0 0.7 constant_dynamic-update-slice_fusion.6
  59.7 0.7 constant_dynamic-update-slice_fusion.5
  60.4 36.0 %all-gather.3.cloned.1.call-done = bf16[128,2,4096]{0,2,1:T(8,128)(2,1)} async-done(((bf16[128,2,64]{0,2,1:T(8,128)(2,1)}), bf16[128,2,4096]{0,2,1:T(8,128)(2,1)}) %all-gather.3.cloned.1.call-update) | async-done | bytes 2097168 | tf_op jit(solution)/shard_map/all_gather | solution.py:145
  96.4 2.9 %multiply_convert_fusion = bf16[128,2,4096]{0,2,1:T(8,128)(2,1)} fusion(bf16[128,2,4096]{0,2,1:T(8,128)(2,1)} %all-gather.3.cloned.1.call-done, f32[4096]{0:T(1024)S(1)} %convert_element_type.96, f32[128,2]{0,1:T(2,128)S(1)} %add_rsqrt_fusion.1), kind=kLoop, calls=%fused_computation | loop fusion | flops 4194304 | bytes 4211712 | tf_op jit(solution)/shard_map/convert_element_type | solution.py:152
  99.3 6.2 %copy.63 = bf16[128,2,4096]{2,1,0:T(2,128)(2,1)} copy(bf16[128,2,4096]{0,2,1:T(8,128)(2,1)} %multiply_convert_fusion) | data formatting | bytes 4194304 | tf_op jit(solution)/shard_map/convert_element_type | solution.py:152
  105.5 4.1 %reshape.228 = bf16[256,4096]{1,0:T(8,128)(2,1)} reshape(bf16[128,2,4096]{2,1,0:T(2,128)(2,1)} %copy.63) | data formatting | bytes 4194304 | tf_op jit(solution)/shard_map/reshape | solution.py:152
  109.7 2.9 %fusion.3 = bf16[256,192]{0,1:T(8,128)(2,1)S(1)} fusion(bf16[256,4096]{1,0:T(8,128)(2,1)} %reshape.228, bf16[4096,192]{0,1:T(8,128)(2,1)} %get-tuple-element.21, bf16[4096,192]{0,1:T(8,128)(2,1)} %constant_dynamic-update-slice_fusion.5, pred[]{:T(512)S(6)} %eq.2), kind=kOutput, calls=%fused_computation.6 | convolution fusion | flops 403488768 | bytes 5341185 | tf_op jit(solution)/shard_map/dot_general | solution.py:160
  112.6 0.1 copy.64
  112.7 0.7 reshape.229
  113.4 8.5 %all-to-all-start = ((bf16[128,2,192]{2,1,0:T(2,128)(2,1)}), bf16[128,2,192]{2,1,0:T(2,128)(2,1)S(1)}, u32[]{:S(2)}, u32[]{:S(2)}) async-start(bf16[128,2,192]{2,1,0:T(2,128)(2,1)} %reshape.229), calls=%async_computation | async-start | bytes 262144 | tf_op jit(solution)/shard_map/all_to_all | solution.py:162
  122.0 0.0 all-gather.5.cloned.1.call-start
  122.0 0.1 multiply_cosine_fusion
  122.1 11.4 %all-to-all-done = bf16[128,2,192]{2,1,0:T(2,128)(2,1)S(1)} async-done(((bf16[128,2,192]{2,1,0:T(2,128)(2,1)}), bf16[128,2,192]{2,1,0:T(2,128)(2,1)S(1)}, u32[]{:S(2)}, u32[]{:S(2)}) %all-to-all-start) | async-done | bytes 98336 | tf_op jit(solution)/shard_map/all_to_all | solution.py:162
  133.6 0.1 broadcast_select_fusion.1
  133.7 8.2 %collective-permute-start.1 = (bf16[2,2,64,96]{3,2,1,0:T(8,128)(2,1)S(1)}, bf16[2,2,64,96]{3,2,1,0:T(8,128)(2,1)S(1)}, u32[]{:S(2)}, u32[]{:S(2)}) collective-permute-start(bf16[2,2,64,96]{3,2,1,0:T(8,128)(2,1)S(1)} %get-tuple-element.27), channel_id=1, source_target_pairs={{0,1},{1,0},{2,3},{3,2},{4,5},{5,4},{6,7},{7,6},{8,9},{9,8},{10,11... | collective-permute-start | bytes 147464 | tf_op jit(solution)/shard_map/ppermute | solution.py:23
  141.9 0.1 multiply_exponential_fusion
  141.9 0.8 collective-permute-done.1
  142.8 0.1 slice_convert_fusion
  142.9 0.1 fusion.19
  143.0 0.1 reshape.234
  143.2 0.1 reshape.235
  143.3 0.1 reshape.230
  143.4 0.1 fusion.20
  143.6 0.1 fusion.10
  143.7 0.2 convolution_multiply_fusion
  143.9 0.2 fusion.13
  144.1 1.2 fusion.15
  145.3 0.1 fusion.7
  145.4 0.1 reshape.233
  145.6 0.1 fusion.9
  145.7 20.6 %all_gather.10 = bf16[8,2,4,2048]{3,2,1,0:T(4,128)(2,1)} all-gather(bf16[1,2,4,2048]{3,2,1,0:T(4,128)(2,1)S(1)} %broadcast_in_dim_reshape.3), channel_id=1, replica_groups=mesh['dp'=4,'kv_0'=8,'kv_1'=8,'tp'=2] {'kv_0'}, dimensions={0}, use_global_device_ids=true | all-gather | bytes 294912 | tf_op jit(solution)/shard_map/all_gather | solution.py:35
  166.3 0.0 all-gather.5.cloned.1.call-update
  166.3 0.6 copy.78
  167.0 37.0 %all-gather.5.cloned.1.call-done = bf16[64,2,4,2048]{3,2,1,0:T(4,128)(2,1)} async-done(((bf16[8,2,4,2048]{3,2,1,0:T(4,128)(2,1)}), bf16[64,2,4,2048]{3,2,1,0:T(4,128)(2,1)}) %all-gather.5.cloned.1.call-update) | async-done | bytes 2097168 | tf_op jit(solution)/shard_map/all_gather | solution.py:35
  204.0 2.7 %copy.110 = bf16[64,2,4,2048]{3,0,2,1:T(8,128)(2,1)S(1)} copy(bf16[64,2,4,2048]{3,2,1,0:T(4,128)(2,1)} %all-gather.5.cloned.1.call-done) | data formatting | bytes 4194304 | tf_op jit(solution)/shard_map/all_gather | solution.py:35
  206.7 2.2 copy.76
  208.9 2.2 dot_general.25
  211.1 2.3 %convolution_convert_fusion = bf16[128,4,64]{0,2,1:T(8,128)(2,1)S(1)} fusion(bf16[128,4,2048]{2,0,1:T(8,128)(2,1)} %dot_general.25, bf16[2048,64]{0,1:T(8,128)(2,1)S(1)} %copy-done), kind=kOutput, calls=%fused_computation.7 | convolution fusion | flops 134250496 | bytes 2424832 | tf_op jit(solution)/shard_map/dot_general | solution.py:197
  213.5 8.3 %all_to_all.20 = bf16[2,128,4,32]{1,3,2,0:T(8,128)(2,1)S(1)} all-to-all(bf16[2,128,4,32]{1,3,2,0:T(8,128)(2,1)S(1)} %bitcast.46), channel_id=1, replica_groups=mesh['dp'=4,'kv_0'=8,'kv_1'=8,'tp'=2] {'tp'}, dimensions={0} | all-to-all | bytes 131072 | tf_op jit(solution)/shard_map/all_to_all | solution.py:53
  221.8 0.6 reduce_sum.32
  (41 shorter events, 0.3 us)
Async XLA Ops:
  7.2 204.0 %copy-start = (bf16[2048,64]{0,1:T(8,128)(2,1)S(1)}, bf16[2048,64]{0,1:T(8,128)(2,1)}, u32[]{:S(2)}) copy-start(bf16[2048,64]{0,1:T(8,128)(2,1)} %param.19) | copy-start | bytes 786436
  7.2 12.5 %copy-start.6 = (bf16[128,4,64]{0,2,1:T(8,128)(2,1)S(1)}, bf16[128,4,64]{0,2,1:T(8,128)(2,1)}, u32[]{:S(2)}) copy-start(bf16[128,4,64]{0,2,1:T(8,128)(2,1)} %param.13) | copy-start | bytes 196612
  7.2 12.6 %copy-start.4 = (bf16[4096,16]{0,1:T(8,128)(2,1)S(1)}, bf16[4096,16]{0,1:T(8,128)(2,1)}, u32[]{:S(2)}) copy-start(bf16[4096,16]{0,1:T(8,128)(2,1)} %param.15) | copy-start | bytes 393220
  7.2 42.9 %copy-start.5 = (bf16[4096,16]{0,1:T(8,128)(2,1)S(1)}, bf16[4096,16]{0,1:T(8,128)(2,1)}, u32[]{:S(2)}) copy-start(bf16[4096,16]{0,1:T(8,128)(2,1)} %param.16) | copy-start | bytes 393220
  7.2 43.6 %copy-start.2 = (bf16[4096,32]{0,1:T(8,128)(2,1)S(1)}, bf16[4096,32]{0,1:T(8,128)(2,1)}, u32[]{:S(2)}) copy-start(bf16[4096,32]{0,1:T(8,128)(2,1)} %param.17) | copy-start | bytes 786436
  7.2 13.2 %copy-start.12 = (s32[2]{0:T(128)S(1)}, s32[2]{0:T(128)}, u32[]{:S(2)}) copy-start(s32[2]{0:T(128)} %param.24) | copy-start | bytes 28
  7.2 13.3 %copy-start.11 = (s32[2]{0:T(128)S(1)}, s32[2]{0:T(128)}, u32[]{:S(2)}) copy-start(s32[2]{0:T(128)} %param.25) | copy-start | bytes 28
  7.2 13.3 %copy-start.13 = (f32[8]{0:T(128)S(1)}, f32[8]{0:T(128)}, u32[]{:S(2)}) copy-start(f32[8]{0:T(128)} %param.20) | copy-start | bytes 100
  7.3 13.6 %copy-start.9 = (bf16[2,4,8,128]{3,2,1,0:T(8,128)(2,1)S(1)}, bf16[2,4,8,128]{3,2,1,0:T(8,128)(2,1)}, u32[]{:S(2)}) copy-start(bf16[2,4,8,128]{3,2,1,0:T(8,128)(2,1)} %param.22) | copy-start | bytes 49156
  7.3 13.7 %copy-start.10 = (bf16[4096]{0:T(1024)(128)(2,1)S(1)}, bf16[4096]{0:T(1024)(128)(2,1)}, u32[]{:S(2)}) copy-start(bf16[4096]{0:T(1024)(128)(2,1)} %param.14) | copy-start | bytes 24580
  7.3 44.3 %copy-start.8 = (bf16[2,4,8,256]{3,2,1,0:T(8,128)(2,1)S(1)}, bf16[2,4,8,256]{3,2,1,0:T(8,128)(2,1)}, u32[]{:S(2)}) copy-start(bf16[2,4,8,256]{3,2,1,0:T(8,128)(2,1)} %param.23) | copy-start | bytes 98308
  7.3 89.1 %all-gather.3.cloned.1.call-start = ((), (), s32[]{:S(2)}) async-start(), calls=%async_computation.2 | async-start | bytes 2129920 | tf_op jit(solution)/shard_map/all_gather | solution.py:145
  11.0 44.2 %collective-permute-start = (bf16[4096,96]{0,1:T(8,128)(2,1)}, bf16[4096,96]{0,1:T(8,128)(2,1)}, u32[]{:S(2)}, u32[]{:S(2)}) collective-permute-start(bf16[4096,96]{0,1:T(8,128)(2,1)} %pad_maximum_fusion), channel_id=1, source_target_pairs={{0,1},{1,0},{2,3},{3,2},{4,5},{5,4},{6,7},{7,6},{8,9},{9,8},{10,11... | collective-permute-start | bytes 2359304 | tf_op jit(solution)/shard_map/ppermute | solution.py:23
  51.5 2.8 %copy-start.3 = (bf16[4096,32]{0,1:T(8,128)(2,1)S(1)}, bf16[4096,32]{0,1:T(8,128)(2,1)}, u32[]{:S(2)}) copy-start(bf16[4096,32]{0,1:T(8,128)(2,1)} %param.18) | copy-start | bytes 786436
  54.4 89.7 %copy-start.1 = (f32[2,8,128,256]{3,2,1,0:T(8,128)}, f32[2,8,128,256]{3,2,1,0:T(8,128)S(1)}, u32[]{:S(2)}) copy-start(f32[2,8,128,256]{3,2,1,0:T(8,128)S(1)} %multiply_add_fusion) | copy-start | bytes 6291460
  113.4 20.1 %all-to-all-start = ((bf16[128,2,192]{2,1,0:T(2,128)(2,1)}), bf16[128,2,192]{2,1,0:T(2,128)(2,1)S(1)}, u32[]{:S(2)}, u32[]{:S(2)}) async-start(bf16[128,2,192]{2,1,0:T(2,128)(2,1)} %reshape.229), calls=%async_computation | async-start | bytes 262144 | tf_op jit(solution)/shard_map/all_to_all | solution.py:162
  122.0 82.0 %all-gather.5.cloned.1.call-start = ((), (), s32[]{:S(2)}) async-start(), calls=%async_computation.3 | async-start | bytes 2359296 | tf_op jit(solution)/shard_map/all_gather | solution.py:35
  133.7 9.1 %collective-permute-start.1 = (bf16[2,2,64,96]{3,2,1,0:T(8,128)(2,1)S(1)}, bf16[2,2,64,96]{3,2,1,0:T(8,128)(2,1)S(1)}, u32[]{:S(2)}, u32[]{:S(2)}) collective-permute-start(bf16[2,2,64,96]{3,2,1,0:T(8,128)(2,1)S(1)} %get-tuple-element.27), channel_id=1, source_target_pairs={{0,1},{1,0},{2,3},{3,2},{4,5},{5,4},{6,7},{7,6},{8,9},{9,8},{10,11... | collective-permute-start | bytes 147464 | tf_op jit(solution)/shard_map/ppermute | solution.py:23
  143.4 2.0 copy-start.7
Sparse Core Ops, SparseCore 0:
  11.7 84.6 all-gather.2
  166.5 37.4 all-gather.4
where the time goes:
time: 230 us; the launch traced here: 229 us
  waiting for transfers between devices  85.2 us (37%)
  blocking collectives  58 us (25%)
  local copies, waits for them, and re-layouts  29.3 us (13%)
  starting transfers between devices  25.6 us (11%)
  between operations  14.4 us (6%)
  matrix products  9.71 us (4%)
  other arithmetic  7.02 us (3%)
    all_gather x1, waiting for transfers between devices, stacked_from(): blocks = lax.all_gather(blocks, axes[k], axis=0, tiled=True)  37 us
    all_gather x1, waiting for transfers between devices, shards(): gathered = lax.all_gather(own_half, KV, axis=2, tiled=True)  36 us
    psum x2, blocking collectives, over_axes(): value = lax.psum(value, axis)  29.1 us
    all_gather x1, blocking collectives, stacked_from(): blocks = lax.all_gather(blocks, axes[k], axis=0, tiled=True)  20.6 us
    ppermute x2, starting transfers between devices, swapped(): lax.ppermute(value, axis, [(i, i ^ 1 << bit) for i in range(lax.axis_size...  16.9 us
    all_to_all x1, waiting for transfers between devices, shards(): lax.all_to_all(columns, KV, split_axis=0, concat_axis=2, tiled=True)  11.4 us
    all_to_all x1, starting transfers between devices, shards(): lax.all_to_all(columns, KV, split_axis=0, concat_axis=2, tiled=True)  8.55 us
    all_to_all x1, blocking collectives, summed_on_arrival(): lax.all_to_all(in_blocks(value, dim, length), axis, 0, 0, tiled=True)  8.27 us
  transfers between devices with their start and end apart: 5, of which 4 were waited for; matrix products, arithmetic and copies ran while one was open for 6% of the time, Pallas kernels for 0%

commit v1 on v0

v1 whole, which is shorter than its diff:
```python
import functools

import jax
import jax.numpy as jnp
from jax import lax
from jax.experimental import pallas as pl
from jax.experimental.pallas import tpu as pltpu
from jax.sharding import Mesh
from jax.sharding import PartitionSpec as P

KV = ("kv_0", "kv_1")
TP_KV = ("tp", "kv_0", "kv_1")
DP_KV = ("dp", "kv_0", "kv_1")
KV_TP = ("kv_0", "kv_1", "tp")
MESH = pl.DeviceIdType.MESH
F32, BF16 = jnp.float32, jnp.bfloat16

epsilon = 1e-06


def ring_place(i, n):
    odd = lax.rem(i, 2)
    return odd * ((i + 1) // 2) + (1 - odd) * lax.rem(n - i // 2, n)


class TorusGather:
    def __init__(self, own, held, arrived, first_sent, ring_sent, nz, ny):
        self.own, self.held, self.arrived = own, held, arrived
        self.first_sent, self.ring_sent = first_sent, ring_sent
        z, y = lax.axis_index("kv_0"), lax.axis_index("kv_1")
        self.partner = {"tp": 1 - lax.axis_index("tp")}
        self.first = ((y, ny, "kv_1"), (z, nz, "kv_0"))
        self.second = ((z, nz, "kv_0"), (y, ny, "kv_1"))

    def at(self, ref, p, f, s):
        return ref.at[p, s, f] if p == 0 else ref.at[p, f, s]

    def copy(self, p, f, s, source, sent, device):
        return pltpu.make_async_remote_copy(
            src_ref=source,
            dst_ref=self.at(self.held, p, f, s),
            send_sem=sent,
            recv_sem=self.at(self.arrived, p, f, s),
            device_id=device,
            device_id_type=MESH,
        )

    def wait(self, p, f, s):
        chunk = self.at(self.held, p, f, s)
        self.copy(p, f, s, chunk, self.first_sent.at[0, 0], self.partner).wait_recv()

    def first_copy(self, p, d):
        (f, n, axis), (s, _, _) = self.first[p], self.second[p]
        return self.copy(
            p, f, s, self.own(p), self.first_sent.at[p, d], {axis: lax.rem(f + d, n)}
        )

    def start_first(self):
        for p in range(2):
            n = self.first[p][1]

            def send(i, _, p=p, n=n):
                self.first_copy(p, ring_place(i, n)).start()
                return 0

            lax.fori_loop(1, n, send, 0)

    def ring_copy(self, p, k, i, way):
        (f, nf, _), (s, ns, axis) = self.first[p], self.second[p]
        other = lax.rem(f + ring_place(i, nf), nf)
        origin = lax.rem(s - way * k + ns, ns)
        chunk = self.at(self.held, p, other, origin)
        if k == 0:
            source = self.own(p) if isinstance(i, int) and i == 0 else chunk
        else:
            source = chunk
        sent = self.ring_sent.at[p, (1 + way) // 2, k, i]
        return self.copy(p, other, origin, source, sent, {axis: lax.rem(s + way + ns, ns)})

    def pass_on(self, k, i, ways):
        for p in range(2):
            (f, nf, _), (s, ns, _) = self.first[p], self.second[p]
            other = lax.rem(f + ring_place(i, nf), nf)
            if k == 0:
                if not (isinstance(i, int) and i == 0):
                    self.wait(p, other, s)
                for way in ways:
                    self.ring_copy(p, k, i, way).start()
            else:
                for way in (1, -1):
                    self.wait(p, other, lax.rem(s - way * k + ns, ns))
                    if way in ways:
                        self.ring_copy(p, k, i, way).start()

    def hops(self):
        return self.second[0][1] // 2

    def start_ring(self):
        self.pass_on(0, 0, (1, -1))

    def loop(self, low, high, step):
        def body(i, _):
            step(i)
            return 0

        lax.fori_loop(low, high, body, 0)

    def round(self, k):
        n = self.first[0][1]
        if k < self.hops() - 1:
            self.loop(1 if k == 0 else 0, n, lambda i: self.pass_on(k, i, (1, -1)))
        else:
            self.loop(0, n // 2, lambda i: self.pass_on(k, i, (1,)))
            self.loop(n // 2, n, lambda i: self.pass_on(k, i, (-1,)))

    def last_arrivals(self):
        k = self.hops()

        def take(i):
            for p in range(2):
                (f, nf, _), (s, ns, _) = self.first[p], self.second[p]
                self.wait(p, lax.rem(f + ring_place(i, nf), nf), lax.rem(s + k, ns))

        self.loop(0, self.first[0][1], take)

    def finish(self):
        n = self.first[0][1]
        for p in range(2):
            self.loop(1, n, lambda d, p=p: self.first_copy(p, d).wait_send())
        for k in range(self.hops()):
            last = k == self.hops() - 1

            def done(i, ways, k=k):
                for p in range(2):
                    for way in ways:
                        self.ring_copy(p, k, i, way).wait_send()

            if last:
                self.loop(0, n // 2, lambda i: done(i, (1,)))
                self.loop(n // 2, n, lambda i: done(i, (-1,)))
            else:
                self.loop(0, n, lambda i: done(i, (1, -1)))


def iota(shape, dim):
    return lax.broadcasted_iota(jnp.int32, shape, dim)


def kernel(
    nz,
    ny,
    tok,
    wq,
    wk,
    wv,
    wg,
    wo,
    prior,
    gain,
    last_k,
    last_v,
    cos_tab,
    sin_tab,
    grid,
    query_decay,
    key_weights,
    carried,
    ret_out,
    state_out,
    keys_out,
    values_out,
    tok_v,
    weights,
    wo_v,
    prior_v,
    state_v,
    state_b,
    tokens_all,
    place,
    order,
    out_a,
    in_a,
    mid,
    out_b,
    in_b,
    rows_f,
    chunk,
    gated_all,
    sent_out,
    got_out,
    ret_v,
    keys_v,
    values_v,
    local,
    tok_arrived,
    tok_first,
    tok_ring,
    gat_arrived,
    gat_first,
    gat_ring,
    pair_sems,
    a_sent,
    a_got,
    b_sent,
    b_got,
):
    z, y, tp = lax.axis_index("kv_0"), lax.axis_index("kv_1"), lax.axis_index("tp")
    heads, seqs = nz, 2 * nz * ny
    kc = wq.shape[0]
    vc = wv.shape[0]
    span = 2 * kc + 2 * vc
    partner = {"tp": 1 - tp}

    loads = [
        pltpu.make_async_copy(tok.at[pl.ds(2 * tp, 2)], tok_v, local.at[0]),
        pltpu.make_async_copy(wq, weights.at[tp, pl.ds(0, kc)], local.at[1]),
        pltpu.make_async_copy(wk, weights.at[tp, pl.ds(kc, kc)], local.at[2]),
        pltpu.make_async_copy(wv, weights.at[tp, pl.ds(2 * kc, vc)], local.at[3]),
        pltpu.make_async_copy(wg, weights.at[tp, pl.ds(2 * kc + vc, vc)], local.at[4]),
        pltpu.make_async_copy(prior, prior_v, local.at[5]),
        pltpu.make_async_copy(wo, wo_v, local.at[6]),
    ]
    for load in loads:
        load.start()

    barrier = pltpu.get_barrier_semaphore()

    def greet(device):
        pl.semaphore_signal(barrier, inc=1, device_id=device, device_id_type=MESH)

    def greet_y(d, _):
        other = lax.rem(y + d, ny)
        greet({"kv_1": other})
        greet({"kv_1": other, "tp": 1 - tp})
        return 0

    def greet_z(d, _):
        greet({"kv_0": lax.rem(z + d, nz)})
        return 0

    lax.fori_loop(1, ny, greet_y, 0)
    lax.fori_loop(1, nz, greet_z, 0)
    greet(partner)
    pl.semaphore_wait(barrier, 2 * (ny - 1) + (nz - 1) + 1)

    loads[0].wait()
    tokens = TorusGather(
        lambda p: tok_v.at[p], tokens_all, tok_arrived, tok_first, tok_ring, nz, ny
    )
    tokens.start_first()
    tokens.start_ring()
    keep = [
        pltpu.make_async_copy(tok_v.at[p], tokens_all.at[p, z, y], local.at[7 + p]) for p in range(2)
    ]
    for each in keep:
        each.start()
    for load in loads[1:5]:
        load.wait()
    swap = pltpu.make_async_remote_copy(
        src_ref=weights.at[tp],
        dst_ref=weights.at[tp],
        send_sem=pair_sems.at[0],
        recv_sem=pair_sems.at[1],
        device_id=partner,
        device_id_type=MESH,
    )
    swap.start()

    loads[5].wait()
    rows = 4 * heads
    head_of = lax.rem(iota((rows, 1), 0), heads)
    for s in range(2):
        weighted = last_k[s].astype(F32) * key_weights[s]
        high = weighted.astype(BF16).astype(F32)
        low = weighted - high

        def one_head(h, _, s=s, high=high, low=low):
            mine = head_of == h
            both = jnp.concatenate([jnp.where(mine, high, 0.0), jnp.where(mine, low, 0.0)], axis=0)
            values = jnp.concatenate([last_v[s], last_v[s]], axis=0)
            update = lax.dot_general(
                both.astype(BF16), values, (((0,), (0,)), ((), ())), preferred_element_type=F32
            )
            at = s * heads + h
            fresh = carried[at] * prior_v[at] + update
            state_v[at] = fresh
            state_b[at] = fresh.astype(BF16)
            return 0

        lax.fori_loop(0, heads, one_head, 0)
    state_store = pltpu.make_async_copy(state_v, state_out, local.at[9])
    state_store.start()

    tokens.round(0)

    key_size, value_size = ny * kc, ny * vc
    lane = iota((128, 2 * key_size + 2 * value_size), 0)
    column = iota((128, 2 * key_size + 2 * value_size), 1)
    for j in range(ny):
        goal = jnp.where(
            lane < kc,
            kc * j + lane,
            jnp.where(
                lane < 2 * kc,
                key_size + kc * j + lane - kc,
                jnp.where(
                    lane < 2 * kc + vc,
                    2 * key_size + vc * j + lane - 2 * kc,
                    2 * key_size + value_size + vc * j + lane - 2 * kc - vc,
                ),
            ),
        )
        hit = (goal == column) & (lane < span)
        place[pl.ds(128 * j, 128)] = jnp.where(hit, 1.0, 0.0).astype(BF16)
    swap.wait()

    def scale_rows(i, _):
        at = pl.ds(pl.multiple_of(i * 16, 16), 16)
        for side in range(2):
            weights[side, at] = (weights[side, at].astype(F32) * gain[...]).astype(BF16)
        return 0

    lax.fori_loop(0, span // 16, scale_rows, 0)
    for k in range(1, tokens.hops()):
        tokens.round(k)
    source = iota((4 * seqs, seqs), 0)
    target = iota((4 * seqs, seqs), 1)
    for p in range(4):
        row_seq = 2 * (source // 8) + lax.rem(source // 2, 2)
        row_prop = 2 * (lax.rem(source, 8) // 4) + lax.rem(source, 2)
        hit = (row_seq == target) & (row_prop == p)
        order[:, pl.ds(seqs * p, seqs)] = jnp.where(hit, 1.0, 0.0).astype(BF16)
    tokens.last_arrivals()
    for each in keep:
        each.wait()

    depth = tok_v.shape[1]
    width = nz * ny * depth
    for p in range(2):
        total = jnp.zeros((2 * span, seqs), F32)
        squares = jnp.zeros((1, seqs), F32)
        for c in range(nz):
            block = tokens_all[p, c].reshape(ny * depth, seqs)
            cut = pl.ds(c * ny * depth, ny * depth)
            total += jnp.dot(
                weights[:, :, cut].reshape(2 * span, ny * depth), block, preferred_element_type=F32
            )
            floats = block.astype(F32)
            squares += jnp.sum(floats * floats, axis=0, keepdims=True)
        scaled = total * lax.rsqrt(squares / width + epsilon)
        for side in range(2):
            part = jnp.concatenate(
                [scaled[side * span : (side + 1) * span], jnp.zeros((128 - span, seqs), F32)], axis=0
            )
            turned = part.T.astype(BF16)
            for to in range(nz):
                out_a[to, side, p] = turned[2 * ny * to : 2 * ny * (to + 1)]

    def a_copy(d):
        to = lax.rem(z + d, nz)
        return pltpu.make_async_remote_copy(
            src_ref=out_a.at[to],
            dst_ref=in_a.at[z],
            send_sem=a_sent.at[d],
            recv_sem=a_got.at[z],
            device_id={"kv_0": to},
            device_id_type=MESH,
        )

    def a_wait(d):
        came = lax.rem(z + d, nz)
        pltpu.make_async_remote_copy(
            src_ref=in_a.at[came],
            dst_ref=in_a.at[came],
            send_sem=a_sent.at[0],
            recv_sem=a_got.at[came],
            device_id=partner,
            device_id_type=MESH,
        ).wait_recv()

    tokens.loop(1, nz, lambda d: a_copy(d).start())
    own_a = pltpu.make_async_copy(out_a.at[z], in_a.at[z], local.at[10])
    own_a.start()
    own_a.wait()
    tokens.loop(1, nz, a_wait)

    mid[...] = in_a[...].reshape(nz * 4 * 2 * ny, 128).astype(F32)
    stride = 4 * 2 * ny
    for to in range(ny):
        for side in range(2):
            for s in range(2):
                parts = [
                    mid[pl.ds(side * 4 * ny + p * 2 * ny + 2 * to + s, nz, stride=stride), :]
                    for p in range(2)
                ]
                out_b[to, side, s] = jnp.concatenate(parts, axis=0).astype(BF16)

    def b_copy(d, same):
        to = lax.rem(y + d, ny)
        side = tp if same else 1 - tp
        return pltpu.make_async_remote_copy(
            src_ref=out_b.at[to, side],
            dst_ref=in_b.at[y, tp],
            send_sem=b_sent.at[d, side],
            recv_sem=b_got.at[y, tp],
            device_id={"kv_1": to, "tp": side},
            device_id_type=MESH,
        )

    def b_wait(d, same):
        came = lax.rem(y + d, ny)
        side = tp if same else 1 - tp
        pltpu.make_async_remote_copy(
            src_ref=in_b.at[came, side],
            dst_ref=in_b.at[came, side],
            send_sem=b_sent.at[0, 0],
            recv_sem=b_got.at[came, side],
            device_id=partner,
            device_id_type=MESH,
        ).wait_recv()

    def b_start(d):
        b_copy(d, True).start()
        b_copy(d, False).start()

    tokens.loop(1, ny, b_start)
    b_copy(0, False).start()
    own_b = pltpu.make_async_copy(out_b.at[y, tp], in_b.at[y, tp], local.at[11])
    own_b.start()
    own_b.wait()
    b_wait(0, False)

    def b_take(d):
        b_wait(d, True)
        b_wait(d, False)

    tokens.loop(1, ny, b_take)

    count = 8 * heads
    packed = jnp.concatenate([in_b[j].reshape(count, 128) for j in range(ny)], axis=1)
    fields = jnp.dot(packed, place[...], preferred_element_type=F32)
    query = fields[:, :key_size]
    key = fields[:, key_size : 2 * key_size]
    value = fields[:, 2 * key_size : 2 * key_size + value_size]
    gate = fields[:, 2 * key_size + value_size :]
    cosine, sine = cos_tab[...], sin_tab[...]
    half = key_size // 2

    def turned_by(x):
        swapped = jnp.concatenate([x[:, half:], x[:, :half]], axis=1)
        return x * cosine + swapped * sine

    query_rot = turned_by(query).astype(BF16)
    key_f = turned_by(key) * key_size ** (-0.5)
    key_rot = key_f.astype(BF16)
    value_b = value.astype(BF16)
    scores = lax.dot_general(
        query_rot, key_rot, (((1,), (1,)), ((), ())), preferred_element_type=F32
    )
    inner = jnp.dot((scores * grid[...]).astype(BF16), value_b, preferred_element_type=F32)
    decayed = query_rot.astype(F32) * query_decay[...]
    row = iota((count, 1), 0)
    row_at = lax.rem(row // (2 * heads), 2) * heads + lax.rem(row, heads)
    spread = jnp.concatenate(
        [jnp.where(row_at == at, decayed, 0.0).astype(BF16) for at in range(2 * heads)], axis=1
    )
    states = state_b[...].reshape(2 * heads * key_size, value_size)
    heads_out = inner + jnp.dot(spread, states, preferred_element_type=F32)
    normed = heads_out * lax.rsqrt(jnp.mean(heads_out * heads_out, axis=-1, keepdims=True) + epsilon)
    product = gate / (1.0 + jnp.exp(-gate)) * normed
    for c in range(value_size // 128):
        rows_f[c] = product[:, 128 * c : 128 * (c + 1)]
    for i in range(8):
        prop, seq = 2 * (i // 4) + i % 2, (i // 2) % 2
        keys_v[seq, prop] = key_f[i * heads : (i + 1) * heads].astype(BF16)
        values_v[seq, prop] = value[i * heads : (i + 1) * heads].astype(BF16)
    cut = heads * value_size // 2
    for h in range(heads):
        part, at = divmod(h * value_size, cut)
        for c in range(value_size // 128):
            piece = rows_f[c, pl.ds(h, 8, stride=heads), :]
            chunk[part, :, at + 128 * c : at + 128 * (c + 1)] = piece.astype(BF16)
    small = [
        pltpu.make_async_copy(keys_v, keys_out, local.at[12]),
        pltpu.make_async_copy(values_v, values_out, local.at[13]),
    ]
    for each in small:
        each.start()

    gated = TorusGather(
        lambda p: chunk.at[p], gated_all, gat_arrived, gat_first, gat_ring, nz, ny
    )
    gated.start_first()
    gated.start_ring()
    keep = [
        pltpu.make_async_copy(chunk.at[p], gated_all.at[p, z, y], local.at[14 + p]) for p in range(2)
    ]
    for each in keep:
        each.start()
    for k in range(gated.hops()):
        gated.round(k)
    gated.last_arrivals()
    for each in keep:
        each.wait()
    loads[6].wait()
    total = jnp.zeros((wo_v.shape[0], 4 * seqs), F32)
    for part in range(2):
        total += lax.dot_general(
            wo_v[:, part * cut : (part + 1) * cut],
            gated_all[part].reshape(4 * seqs, cut),
            (((1,), (1,)), ((), ())),
            preferred_element_type=F32,
        )
    rounded = total.astype(BF16)
    mine = rounded.shape[0] // 2
    sent_out[0] = rounded[:mine]
    sent_out[1] = rounded[mine:]
    trade = pltpu.make_async_remote_copy(
        src_ref=sent_out.at[1 - tp],
        dst_ref=got_out,
        send_sem=pair_sems.at[2],
        recv_sem=pair_sems.at[3],
        device_id=partner,
        device_id_type=MESH,
    )
    trade.start()
    trade.wait()
    summed = (sent_out[tp].astype(F32) + got_out[...].astype(F32)).astype(BF16)
    result = jnp.dot(summed, order[...], preferred_element_type=F32).astype(BF16)
    for p in range(4):
        ret_v[p] = result[:, p * seqs : (p + 1) * seqs]
    last = pltpu.make_async_copy(ret_v, ret_out, local.at[16])
    last.start()
    tokens.finish()
    gated.finish()
    tokens.loop(1, nz, lambda d: a_copy(d).wait_send())

    def b_done(d):
        b_copy(d, True).wait_send()
        b_copy(d, False).wait_send()

    tokens.loop(1, ny, b_done)
    b_copy(0, False).wait_send()
    for each in small:
        each.wait()
    state_store.wait()
    last.wait()


def shards(
    nz,
    ny,
    tokens,
    norm_gain,
    query_weight,
    key_weight,
    value_weight,
    gate_weight,
    out_weight,
    decay_rate,
    prior_state,
    last_keys,
    last_values,
    accepted,
    lengths,
):
    _, heads, key_size, value_size = prior_state.shape
    seqs, _, depth = tokens.shape
    width = norm_gain.shape[0]
    kc, vc = query_weight.shape[1], value_weight.shape[1]
    span = 2 * kc + 2 * vc
    log_decay = -decay_rate
    count = 8 * heads

    def to_rows(table):
        table = table.reshape(2, 2, 2, heads, table.shape[-1])
        return table.transpose(1, 0, 2, 3, 4).reshape(count, -1)

    half = key_size // 2
    steps = jnp.arange(4, dtype=jnp.int32)
    positions = (lengths + accepted)[:, None] + steps[None, :]
    frequency = jnp.power(10000.0, -jnp.arange(half, dtype=F32) / half)
    angles = positions.astype(F32)[:, :, None] * frequency
    cosine, sine = jnp.cos(angles), jnp.sin(angles)

    def all_heads(table):
        return to_rows(jnp.broadcast_to(table[:, :, None, :], (2, 4, heads, key_size)))

    cos_tab = all_heads(jnp.concatenate([cosine, cosine], axis=-1))
    sin_tab = all_heads(jnp.concatenate([-sine, sine], axis=-1))
    row = jnp.arange(count, dtype=jnp.int32)
    row_prop = 2 * (row // (4 * heads)) + (row // heads) % 2
    row_seq = (row // (2 * heads)) % 2
    row_head = row % heads
    row_decay = jnp.tile(log_decay, 8)
    offset = (row_prop[:, None] - row_prop[None, :]).astype(F32)
    same = (row_seq[:, None] == row_seq[None, :]) & (row_head[:, None] == row_head[None, :])
    grid = jnp.where(
        same & (offset >= 0.0), jnp.exp(row_decay[:, None] * jnp.maximum(offset, 0.0)), 0.0
    )
    query_decay = jnp.broadcast_to(
        jnp.exp(row_decay * (row_prop.astype(F32) + 1.0))[:, None], (count, key_size)
    )
    power = jnp.maximum(accepted[:, None] - 1 - steps[None, :], 0).astype(F32)
    taken = steps[None, :] < accepted[:, None]
    weight = jnp.where(
        taken[:, :, None], jnp.exp(log_decay[None, None, :] * power[:, :, None]), 0.0
    )
    key_weights = jnp.broadcast_to(
        weight.reshape(2, 4 * heads, 1), (2, 4 * heads, key_size)
    )
    carried = jnp.exp(log_decay[None, :] * accepted[:, None].astype(F32)).reshape(2 * heads)

    any_ref = pl.BlockSpec(memory_space=pl.ANY)
    vmem = pl.BlockSpec(memory_space=pltpu.VMEM)
    smem = pl.BlockSpec(memory_space=pltpu.SMEM)
    dma = pltpu.SemaphoreType.DMA
    cut = heads * value_size // 2
    out_cols = out_weight.shape[1]
    retained, state, new_keys, new_values = pl.pallas_call(
        functools.partial(kernel, nz, ny),
        out_shape=(
            jax.ShapeDtypeStruct((4, out_cols // 2, seqs), BF16),
            jax.ShapeDtypeStruct((2 * heads, key_size, value_size), F32),
            jax.ShapeDtypeStruct((2, 4, heads, key_size), BF16),
            jax.ShapeDtypeStruct((2, 4, heads, value_size), BF16),
        ),
        in_specs=[any_ref] * 7 + [vmem] * 8 + [smem],
        out_specs=(any_ref,) * 4,
        scratch_shapes=[
            pltpu.VMEM((2, depth, seqs), BF16),
            pltpu.VMEM((2, span, width), BF16),
            pltpu.VMEM((out_cols, heads * value_size), BF16),
            pltpu.VMEM((2 * heads, key_size, value_size), F32),
            pltpu.VMEM((2 * heads, key_size, value_size), F32),
            pltpu.VMEM((2 * heads, key_size, value_size), BF16),
            pltpu.VMEM((2, nz, ny, depth, seqs), BF16),
            pltpu.VMEM((128 * ny, 2 * key_size + 2 * value_size), BF16),
            pltpu.VMEM((4 * seqs, 4 * seqs), BF16),
            pltpu.VMEM((nz, 2, 2, 2 * ny, 128), BF16),
            pltpu.VMEM((nz, 2, 2, 2 * ny, 128), BF16),
            pltpu.VMEM((nz * 8 * ny, 128), F32),
            pltpu.VMEM((ny, 2, 2, 2 * nz, 128), BF16),
            pltpu.VMEM((ny, 2, 2, 2 * nz, 128), BF16),
            pltpu.VMEM((value_size // 128, count, 128), F32),
            pltpu.VMEM((2, 8, cut), BF16),
            pltpu.VMEM((2, nz, ny, 8, cut), BF16),
            pltpu.VMEM((2, out_cols // 2, 4 * seqs), BF16),
            pltpu.VMEM((out_cols // 2, 4 * seqs), BF16),
            pltpu.VMEM((4, out_cols // 2, seqs), BF16),
            pltpu.VMEM((2, 4, heads, key_size), BF16),
            pltpu.VMEM((2, 4, heads, value_size), BF16),
            dma((17,)),
            dma((2, nz, ny)),
            dma((2, max(nz, ny))),
            dma((2, 2, nz // 2, ny)),
            dma((2, nz, ny)),
            dma((2, max(nz, ny))),
            dma((2, 2, nz // 2, ny)),
            dma((4,)),
            dma((nz,)),
            dma((nz,)),
            dma((ny, 2)),
            dma((ny, 2)),
        ],
        compiler_params=pltpu.CompilerParams(
            collective_id=0, has_side_effects=True, vmem_limit_bytes=48 * 1024 * 1024
        ),
    )(
        tokens.transpose(1, 2, 0),
        query_weight.T,
        key_weight.T,
        value_weight.T,
        gate_weight.T,
        out_weight.T,
        prior_state.reshape(2 * heads, key_size, value_size),
        norm_gain.astype(F32)[None, :],
        last_keys.reshape(2, 4 * heads, key_size),
        last_values.reshape(2, 4 * heads, value_size),
        cos_tab,
        sin_tab,
        grid,
        query_decay,
        key_weights,
        carried,
    )
    return (
        retained.transpose(2, 0, 1),
        state.reshape(prior_state.shape),
        new_keys,
        new_values,
    )


def solution(mesh):
    nz = ny = 8
    finer = Mesh(
        mesh.devices.reshape(mesh.shape["dp"], nz, ny, mesh.shape["tp"]),
        ("dp", "kv_0", "kv_1", "tp"),
    )
    return jax.shard_map(
        functools.partial(shards, nz, ny),
        mesh=finer,
        in_specs=(
            P("dp", None, KV),
            P(),
            P(None, TP_KV),
            P(None, TP_KV),
            P(None, TP_KV),
            P(None, TP_KV),
            P("tp", KV),
            P("tp"),
            P(DP_KV, "tp", None, None),
            P(DP_KV, None, "tp", None),
            P(DP_KV, None, "tp", None),
            P(DP_KV),
            P(DP_KV),
        ),
        out_specs=(
            P("dp", None, KV_TP),
            P(DP_KV, "tp", None, None),
            P(DP_KV, None, "tp", None),
            P(DP_KV, None, "tp", None),
        ),
        check_vma=False,
    )
```

time: 230 us -> 94.5 us (0.41)
  waiting for transfers between devices: 85.2 us -> 0 us
  Pallas kernels: 0 us -> 77.5 us
  blocking collectives: 58 us -> 0 us
  starting transfers between devices: 25.6 us -> 0 us
  local copies, waits for them, and re-layouts: 29.3 us -> 12.4 us
  between operations: 14.4 us -> 0.71 us
  matrix products: 9.71 us -> 0 us
  other arithmetic: 7.02 us -> 3.42 us
    pallas_call x0 -> x1, Pallas kernels: none -> 77.5 us  [shards(): pl.pallas_call(functools.partial(kernel, nz, ny), out_shape=(jax.ShapeDty...]
    all_gather x2 -> x0, waiting for transfers between devices: 73 us -> none  [the longest x1 37 us: stacked_from(): blocks = lax.all_gather(blocks, axes[k], axis=0, tiled=True)]
    psum x2 -> x0, blocking collectives: 29.1 us -> none  [over_axes(): value = lax.psum(value, axis)]
    all_gather x1 -> x0, blocking collectives: 20.6 us -> none  [stacked_from(): blocks = lax.all_gather(blocks, axes[k], axis=0, tiled=True)]
    ppermute x2 -> x0, starting transfers between devices: 16.9 us -> none  [swapped(): lax.ppermute(value, axis, [(i, i ^ 1 << bit) for i in range(lax.axis_size...]
    all_to_all x1 -> x0, waiting for transfers between devices: 11.4 us -> none  [shards(): lax.all_to_all(columns, KV, split_axis=0, concat_axis=2, tiled=True)]
    dot_general x6 -> x0, matrix products: 9.71 us -> none  [the longest x1 2.89 us: shards(): jnp.dot(normed, both_weights, preferred_element_type=jnp.float32)]
    all_to_all x1 -> x0, starting transfers between devices: 8.55 us -> none  [shards(): lax.all_to_all(columns, KV, split_axis=0, concat_axis=2, tiled=True)]
  transfers between devices with their start and end apart: 5 -> 0, of which waited for: 4 -> 0; matrix products, arithmetic and copies ran while one was open for 6% -> 0% of each run, Pallas kernels for 0% -> 0%
where the time goes in v1:
time: 94.5 us; the launch traced here: 94 us
  Pallas kernels  77.5 us (82%)
  local copies, waits for them, and re-layouts  12.4 us (13%)
  other arithmetic  3.42 us (4%)
    pallas_call x1, Pallas kernels, shards(): pl.pallas_call(functools.partial(kernel, nz, ny), out_shape=(jax.ShapeDty...  77.5 us
    unnamed x22, local copies, waits for them, and re-layouts  11.7 us

profile of v1, /device:TPU:1, one launch (start us, length us, event | category | flops | bytes accessed | tf_op | source)
XLA Modules:
  0.0 94.0 jit_solution(305804633031034729)
XLA Ops:
  0.6 0.7 neg.16
  1.3 0.7 iota_compare_fusion
  2.0 0.1 broadcast_in_dim.29
  2.1 0.1 broadcast_in_dim.30
  2.2 0.7 fusion.7
  3.0 0.1 multiply_exponential_fusion
  3.0 0.1 exp.28.carried
  3.1 0.1 add_convert_fusion
  3.2 0.1 maximum_convert_fusion
  3.3 0.1 mul.100
  3.4 0.1 mul.102
  3.4 0.1 mul.103
  3.5 0.1 mul.95
  3.6 0.2 fusion.6
  3.8 0.1 pad_maximum_fusion
  3.9 0.7 broadcast_in_dim.33
  4.6 0.1 exponential_select_fusion.grid
  4.7 0.1 broadcast_in_dim.32.key_weights
  4.7 0.1 broadcast_in_dim.28.query_decay
  4.8 0.0 copy-start
  4.8 1.6 %copy-done = f32[2,8,128,256]{3,2,1,0:T(8,128)S(1)} copy-done((f32[2,8,128,256]{3,2,1,0:T(8,128)S(1)}, f32[2,8,128,256]{3,2,1,0:T(8,128)}, u32[]{:S(2)}) %copy-start) | copy-done | bytes 2097176
  6.4 0.0 copy-start.1
  6.4 0.9 %copy-done.1 = bf16[4096,32]{0,1:T(8,128)(2,1)S(1)} copy-done((bf16[4096,32]{0,1:T(8,128)(2,1)S(1)}, bf16[4096,32]{0,1:T(8,128)(2,1)}, u32[]{:S(2)}) %copy-start.1) | copy-done | bytes 262168
  7.4 0.0 copy-start.2
  7.4 0.9 %copy-done.2 = bf16[4096,32]{0,1:T(8,128)(2,1)S(1)} copy-done((bf16[4096,32]{0,1:T(8,128)(2,1)S(1)}, bf16[4096,32]{0,1:T(8,128)(2,1)}, u32[]{:S(2)}) %copy-start.2) | copy-done | bytes 262168
  8.3 0.0 copy-start.3
  8.3 0.9 %copy-done.3 = bf16[2048,64]{0,1:T(8,128)(2,1)S(1)} copy-done((bf16[2048,64]{0,1:T(8,128)(2,1)S(1)}, bf16[2048,64]{0,1:T(8,128)(2,1)}, u32[]{:S(2)}) %copy-start.3) | copy-done | bytes 262168
  9.3 0.0 copy-start.4
  9.3 0.9 copy-done.4
  10.2 0.0 copy-start.5
  10.2 0.9 copy-done.5
  11.1 0.0 copy-start.6
  11.1 0.8 copy-done.6
  11.9 0.0 copy-start.7
  11.9 0.8 copy-done.7
  12.7 0.0 copy-start.8
  12.7 0.7 copy-done.8
  13.4 77.5 %shard_map.156 = (bf16[4,32,128]{2,1,0:T(8,128)(2,1)S(1)}, f32[16,128,256]{2,1,0:T(8,128)S(1)}, bf16[2,4,8,128]{3,2,1,0:T(8,128)(2,1)S(1)}, bf16[2,4,8,256]{3,2,1,0:T(8,128)(2,1)S(1)}) custom-call(bf16[4,64,128]{2,1,0:T(8,128)(2,1)S(1)} %bitcast.28, bf16[16,4096]{1,0:T(8,128)(2,1)S(1)} %bitcast.25, bf16[16,4096]{1,0:T(8,128)(2,1)S(1)} %bitcast.26, ...), custom_call_target="tpu_custom_call" | custom-call | tf_op jit(solution)/shard_map/pallas_call | solution.py:620
  90.9 0.6 copy.21
  91.5 1.3 %copy.22 = f32[2,8,128,256]{3,2,1,0:T(8,128)} copy(f32[2,8,128,256]{3,2,1,0:T(8,128)S(1)} %bitcast.19) | data formatting | bytes 4194304
  92.8 0.6 copy.23
  93.4 0.6 copy.24
  (10 shorter events, 0.1 us)
Async XLA Ops:
  4.8 1.6 %copy-start = (f32[2,8,128,256]{3,2,1,0:T(8,128)S(1)}, f32[2,8,128,256]{3,2,1,0:T(8,128)}, u32[]{:S(2)}) copy-start(f32[2,8,128,256]{3,2,1,0:T(8,128)} %param.21) | copy-start | bytes 6291460
  6.4 0.9 %copy-start.1 = (bf16[4096,32]{0,1:T(8,128)(2,1)S(1)}, bf16[4096,32]{0,1:T(8,128)(2,1)}, u32[]{:S(2)}) copy-start(bf16[4096,32]{0,1:T(8,128)(2,1)} %param.17) | copy-start | bytes 786436
  7.4 0.9 %copy-start.2 = (bf16[4096,32]{0,1:T(8,128)(2,1)S(1)}, bf16[4096,32]{0,1:T(8,128)(2,1)}, u32[]{:S(2)}) copy-start(bf16[4096,32]{0,1:T(8,128)(2,1)} %param.18) | copy-start | bytes 786436
  8.3 0.9 %copy-start.3 = (bf16[2048,64]{0,1:T(8,128)(2,1)S(1)}, bf16[2048,64]{0,1:T(8,128)(2,1)}, u32[]{:S(2)}) copy-start(bf16[2048,64]{0,1:T(8,128)(2,1)} %param.19) | copy-start | bytes 786436
  9.3 0.9 copy-start.4
  10.2 0.9 copy-start.5
  11.1 0.8 copy-start.6
  11.9 0.8 copy-start.7
  12.7 0.7 copy-start.8

commit v2 on v1

--- a/solution.py
+++ b/solution.py
@@ -18,9 +18,15 @@
 epsilon = 1e-06
 
 
+def wrap(i, n):
+    return i & (n - 1)
+
+
 def ring_place(i, n):
-    odd = lax.rem(i, 2)
-    return odd * ((i + 1) // 2) + (1 - odd) * lax.rem(n - i // 2, n)
+    if isinstance(i, int):
+        return (i + 1) // 2 if i % 2 else (n - i // 2) % n
+    odd = i & 1
+    return wrap(odd * ((i + 1) >> 1) + (1 - odd) * (n - (i >> 1)), n)
 
 
 class TorusGather:
@@ -52,7 +58,7 @@
     def first_copy(self, p, d):
         (f, n, axis), (s, _, _) = self.first[p], self.second[p]
         return self.copy(
-            p, f, s, self.own(p), self.first_sent.at[p, d], {axis: lax.rem(f + d, n)}
+            p, f, s, self.own(p), self.first_sent.at[p, d], {axis: wrap(f + d, n)}
         )
 
     def start_first(self):
@@ -67,20 +73,20 @@
 
     def ring_copy(self, p, k, i, way):
         (f, nf, _), (s, ns, axis) = self.first[p], self.second[p]
-        other = lax.rem(f + ring_place(i, nf), nf)
-        origin = lax.rem(s - way * k + ns, ns)
+        other = wrap(f + ring_place(i, nf), nf)
+        origin = wrap(s - way * k + ns, ns)
         chunk = self.at(self.held, p, other, origin)
         if k == 0:
             source = self.own(p) if isinstance(i, int) and i == 0 else chunk
         else:
             source = chunk
         sent = self.ring_sent.at[p, (1 + way) // 2, k, i]
-        return self.copy(p, other, origin, source, sent, {axis: lax.rem(s + way + ns, ns)})
+        return self.copy(p, other, origin, source, sent, {axis: wrap(s + way + ns, ns)})
 
     def pass_on(self, k, i, ways):
         for p in range(2):
             (f, nf, _), (s, ns, _) = self.first[p], self.second[p]
-            other = lax.rem(f + ring_place(i, nf), nf)
+            other = wrap(f + ring_place(i, nf), nf)
             if k == 0:
                 if not (isinstance(i, int) and i == 0):
                     self.wait(p, other, s)
@@ -88,7 +94,7 @@
                     self.ring_copy(p, k, i, way).start()
             else:
                 for way in (1, -1):
-                    self.wait(p, other, lax.rem(s - way * k + ns, ns))
+                    self.wait(p, other, wrap(s - way * k + ns, ns))
                     if way in ways:
                         self.ring_copy(p, k, i, way).start()
 
@@ -105,13 +111,19 @@
 
         lax.fori_loop(low, high, body, 0)
 
-    def round(self, k):
+    def round(self, k, beside=None):
         n = self.first[0][1]
+
+        def both(i, ways):
+            self.pass_on(k, i, ways)
+            if beside is not None:
+                beside(i)
+
         if k < self.hops() - 1:
-            self.loop(1 if k == 0 else 0, n, lambda i: self.pass_on(k, i, (1, -1)))
+            self.loop(1 if k == 0 else 0, n, lambda i: both(i, (1, -1)))
         else:
-            self.loop(0, n // 2, lambda i: self.pass_on(k, i, (1,)))
-            self.loop(n // 2, n, lambda i: self.pass_on(k, i, (-1,)))
+            self.loop(0, n // 2, lambda i: both(i, (1,)))
+            self.loop(n // 2, n, lambda i: both(i, (-1,)))
 
     def last_arrivals(self):
         k = self.hops()
@@ -119,7 +131,7 @@
         def take(i):
             for p in range(2):
                 (f, nf, _), (s, ns, _) = self.first[p], self.second[p]
-                self.wait(p, lax.rem(f + ring_place(i, nf), nf), lax.rem(s + k, ns))
+                self.wait(p, wrap(f + ring_place(i, nf), nf), wrap(s + k, ns))
 
         self.loop(0, self.first[0][1], take)
 
@@ -156,15 +168,13 @@
     wg,
     wo,
     prior,
+    last_k_in,
+    last_v_in,
+    decay_in,
+    accepted_in,
+    lengths_in,
     gain,
-    last_k,
-    last_v,
-    cos_tab,
-    sin_tab,
-    grid,
-    query_decay,
-    key_weights,
-    carried,
+    frequency,
     ret_out,
     state_out,
     keys_out,
@@ -173,7 +183,12 @@
     weights,
     wo_v,
     prior_v,
-    state_v,
+    last_k,
+    last_v,
+    decay,
+    accepted,
+    lengths,
+    weighted_keys,
     state_b,
     tokens_all,
     place,
@@ -188,9 +203,6 @@
     gated_all,
     sent_out,
     got_out,
-    ret_v,
-    keys_v,
-    values_v,
     local,
     tok_arrived,
     tok_first,
@@ -220,7 +232,19 @@
         pltpu.make_async_copy(prior, prior_v, local.at[5]),
         pltpu.make_async_copy(wo, wo_v, local.at[6]),
     ]
-    for load in loads:
+    small_loads = [
+        pltpu.make_async_copy(source, target, local.at[17 + i])
+        for i, (source, target) in enumerate(
+            (
+                (last_k_in, last_k),
+                (last_v_in, last_v),
+                (decay_in, decay),
+                (accepted_in, accepted),
+                (lengths_in, lengths),
+            )
+        )
+    ]
+    for load in loads + small_loads:
         load.start()
 
     barrier = pltpu.get_barrier_semaphore()
@@ -229,13 +253,13 @@
         pl.semaphore_signal(barrier, inc=1, device_id=device, device_id_type=MESH)
 
     def greet_y(d, _):
-        other = lax.rem(y + d, ny)
+        other = wrap(y + d, ny)
         greet({"kv_1": other})
         greet({"kv_1": other, "tp": 1 - tp})
         return 0
 
     def greet_z(d, _):
-        greet({"kv_0": lax.rem(z + d, nz)})
+        greet({"kv_0": wrap(z + d, nz)})
         return 0
 
     lax.fori_loop(1, ny, greet_y, 0)
@@ -266,70 +290,63 @@
     )
     swap.start()
 
+    key_size, value_size = ny * kc, ny * vc
+
     loads[5].wait()
-    rows = 4 * heads
-    head_of = lax.rem(iota((rows, 1), 0), heads)
+    for load in small_loads:
+        load.wait()
+    rows, count = 4 * heads, 8 * heads
+    head_of = iota((rows, 1), 0) & (heads - 1)
+
+    def by_head(shape):
+        head = iota(shape, 0) & (heads - 1)
+        table = jnp.zeros(shape, F32)
+        for h in range(heads):
+            table = jnp.where(head == h, -decay[h], table)
+        return table
+
+    taken_decay = by_head((rows, 128))
+    before = iota((rows, 128), 0) >> (heads.bit_length() - 1)
     for s in range(2):
-        weighted = last_k[s].astype(F32) * key_weights[s]
+        power = jnp.maximum(accepted[s] - 1 - before, 0).astype(F32)
+        key_weights = jnp.where(before < accepted[s], jnp.exp(taken_decay * power), 0.0)
+        weighted = last_k[s].astype(F32) * key_weights
         high = weighted.astype(BF16).astype(F32)
-        low = weighted - high
-
-        def one_head(h, _, s=s, high=high, low=low):
-            mine = head_of == h
-            both = jnp.concatenate([jnp.where(mine, high, 0.0), jnp.where(mine, low, 0.0)], axis=0)
+        weighted_keys[s, 0] = high
+        weighted_keys[s, 1] = weighted - high
+
+    def one_head(h):
+        mine = head_of == h
+        for s in range(2):
+            both = jnp.concatenate(
+                [jnp.where(mine, weighted_keys[s, part], 0.0) for part in range(2)], axis=0
+            )
             values = jnp.concatenate([last_v[s], last_v[s]], axis=0)
             update = lax.dot_general(
                 both.astype(BF16), values, (((0,), (0,)), ((), ())), preferred_element_type=F32
             )
             at = s * heads + h
-            fresh = carried[at] * prior_v[at] + update
-            state_v[at] = fresh
+            power = jnp.full((1, value_size), -decay[h] * accepted[s].astype(F32), F32)
+            fresh = jnp.exp(power) * prior_v[at] + update
+            state_out[at] = fresh
             state_b[at] = fresh.astype(BF16)
-            return 0
-
-        lax.fori_loop(0, heads, one_head, 0)
-    state_store = pltpu.make_async_copy(state_v, state_out, local.at[9])
-    state_store.start()
-
-    tokens.round(0)
-
-    key_size, value_size = ny * kc, ny * vc
-    lane = iota((128, 2 * key_size + 2 * value_size), 0)
-    column = iota((128, 2 * key_size + 2 * value_size), 1)
-    for j in range(ny):
-        goal = jnp.where(
-            lane < kc,
-            kc * j + lane,
-            jnp.where(
-                lane < 2 * kc,
-                key_size + kc * j + lane - kc,
-                jnp.where(
-                    lane < 2 * kc + vc,
-                    2 * key_size + vc * j + lane - 2 * kc,
-                    2 * key_size + value_size + vc * j + lane - 2 * kc - vc,
-                ),
-            ),
-        )
-        hit = (goal == column) & (lane < span)
-        place[pl.ds(128 * j, 128)] = jnp.where(hit, 1.0, 0.0).astype(BF16)
+
+    one_head(0)
+    tokens.round(0, one_head)
+
     swap.wait()
 
-    def scale_rows(i, _):
-        at = pl.ds(pl.multiple_of(i * 16, 16), 16)
-        for side in range(2):
-            weights[side, at] = (weights[side, at].astype(F32) * gain[...]).astype(BF16)
-        return 0
-
-    lax.fori_loop(0, span // 16, scale_rows, 0)
+    blocks = span // 16
+
+    def scale_rows(i):
+        @pl.when(i < blocks)
+        def _():
+            at = pl.ds(pl.multiple_of(i * 16, 16), 16)
+            for side in range(2):
+                weights[side, at] = (weights[side, at].astype(F32) * gain[...]).astype(BF16)
+
     for k in range(1, tokens.hops()):
-        tokens.round(k)
-    source = iota((4 * seqs, seqs), 0)
-    target = iota((4 * seqs, seqs), 1)
-    for p in range(4):
-        row_seq = 2 * (source // 8) + lax.rem(source // 2, 2)
-        row_prop = 2 * (lax.rem(source, 8) // 4) + lax.rem(source, 2)
-        hit = (row_seq == target) & (row_prop == p)
-        order[:, pl.ds(seqs * p, seqs)] = jnp.where(hit, 1.0, 0.0).astype(BF16)
+        tokens.round(k, scale_rows if k == 1 else None)
     tokens.last_arrivals()
     for each in keep:
         each.wait()
@@ -357,7 +374,7 @@
                 out_a[to, side, p] = turned[2 * ny * to : 2 * ny * (to + 1)]
 
     def a_copy(d):
-        to = lax.rem(z + d, nz)
+        to = wrap(z + d, nz)
         return pltpu.make_async_remote_copy(
             src_ref=out_a.at[to],
             dst_ref=in_a.at[z],
@@ -368,7 +385,7 @@
         )
 
     def a_wait(d):
-        came = lax.rem(z + d, nz)
+        came = wrap(z + d, nz)
         pltpu.make_async_remote_copy(
             src_ref=in_a.at[came],
             dst_ref=in_a.at[came],
@@ -381,6 +398,32 @@
     tokens.loop(1, nz, lambda d: a_copy(d).start())
     own_a = pltpu.make_async_copy(out_a.at[z], in_a.at[z], local.at[10])
     own_a.start()
+
+    shift = heads.bit_length() - 1
+
+    def prop_of(i):
+        return 2 * (i >> (shift + 2)) + ((i >> shift) & 1)
+
+    def at_of(i):
+        return ((i >> (shift + 1)) & 1) * heads + (i & (heads - 1))
+
+    row = iota((count, 128), 0)
+    first = jnp.where((row >> (shift + 1)) & 1 == 0, lengths[0] + accepted[0], lengths[1] + accepted[1])
+    angles = (first + prop_of(row)).astype(F32) * frequency[...]
+    cosine = jnp.cos(angles)
+    lane_sign = jnp.where(iota((count, 128), 1) < key_size // 2, -1.0, 1.0)
+    sine = jnp.sin(angles) * lane_sign
+    decays = by_head((count, 128))
+    query_decay = jnp.exp(decays * (prop_of(row) + 1).astype(F32))
+    other = iota((count, count), 1)
+    here = row[:, :count]
+    offset = prop_of(here) - prop_of(other)
+    grid = jnp.where(
+        (at_of(here) == at_of(other)) & (offset >= 0),
+        jnp.exp(decays[:, :count] * jnp.maximum(offset, 0).astype(F32)),
+        0.0,
+    )
+
     own_a.wait()
     tokens.loop(1, nz, a_wait)
 
@@ -396,7 +439,7 @@
                 out_b[to, side, s] = jnp.concatenate(parts, axis=0).astype(BF16)
 
     def b_copy(d, same):
-        to = lax.rem(y + d, ny)
+        to = wrap(y + d, ny)
         side = tp if same else 1 - tp
         return pltpu.make_async_remote_copy(
             src_ref=out_b.at[to, side],
@@ -408,7 +451,7 @@
         )
 
     def b_wait(d, same):
-        came = lax.rem(y + d, ny)
+        came = wrap(y + d, ny)
         side = tp if same else 1 - tp
         pltpu.make_async_remote_copy(
             src_ref=in_b.at[came, side],
@@ -427,6 +470,25 @@
     b_copy(0, False).start()
     own_b = pltpu.make_async_copy(out_b.at[y, tp], in_b.at[y, tp], local.at[11])
     own_b.start()
+
+    lane = iota((128, 2 * key_size + 2 * value_size), 0)
+    column = iota((128, 2 * key_size + 2 * value_size), 1)
+    for j in range(ny):
+        goal = jnp.where(
+            lane < kc,
+            kc * j + lane,
+            jnp.where(
+                lane < 2 * kc,
+                key_size + kc * j + lane - kc,
+                jnp.where(
+                    lane < 2 * kc + vc,
+                    2 * key_size + vc * j + lane - 2 * kc,
+                    2 * key_size + value_size + vc * j + lane - 2 * kc - vc,
+                ),
+            ),
+        )
+        hit = (goal == column) & (lane < span)
+        place[pl.ds(128 * j, 128)] = jnp.where(hit, 1.0, 0.0).astype(BF16)
     own_b.wait()
     b_wait(0, False)
 
@@ -436,14 +498,12 @@
 
     tokens.loop(1, ny, b_take)
 
-    count = 8 * heads
     packed = jnp.concatenate([in_b[j].reshape(count, 128) for j in range(ny)], axis=1)
     fields = jnp.dot(packed, place[...], preferred_element_type=F32)
     query = fields[:, :key_size]
     key = fields[:, key_size : 2 * key_size]
     value = fields[:, 2 * key_size : 2 * key_size + value_size]
     gate = fields[:, 2 * key_size + value_size :]
-    cosine, sine = cos_tab[...], sin_tab[...]
     half = key_size // 2
 
     def turned_by(x):
@@ -457,10 +517,9 @@
     scores = lax.dot_general(
         query_rot, key_rot, (((1,), (1,)), ((), ())), preferred_element_type=F32
     )
-    inner = jnp.dot((scores * grid[...]).astype(BF16), value_b, preferred_element_type=F32)
-    decayed = query_rot.astype(F32) * query_decay[...]
-    row = iota((count, 1), 0)
-    row_at = lax.rem(row // (2 * heads), 2) * heads + lax.rem(row, heads)
+    inner = jnp.dot((scores * grid).astype(BF16), value_b, preferred_element_type=F32)
+    decayed = query_rot.astype(F32) * query_decay
+    row_at = at_of(iota((count, 1), 0))
     spread = jnp.concatenate(
         [jnp.where(row_at == at, decayed, 0.0).astype(BF16) for at in range(2 * heads)], axis=1
     )
@@ -472,20 +531,14 @@
         rows_f[c] = product[:, 128 * c : 128 * (c + 1)]
     for i in range(8):
         prop, seq = 2 * (i // 4) + i % 2, (i // 2) % 2
-        keys_v[seq, prop] = key_f[i * heads : (i + 1) * heads].astype(BF16)
-        values_v[seq, prop] = value[i * heads : (i + 1) * heads].astype(BF16)
+        keys_out[seq, prop] = key_f[i * heads : (i + 1) * heads].astype(BF16)
+        values_out[seq, prop] = value[i * heads : (i + 1) * heads].astype(BF16)
     cut = heads * value_size // 2
     for h in range(heads):
         part, at = divmod(h * value_size, cut)
         for c in range(value_size // 128):
             piece = rows_f[c, pl.ds(h, 8, stride=heads), :]
             chunk[part, :, at + 128 * c : at + 128 * (c + 1)] = piece.astype(BF16)
-    small = [
-        pltpu.make_async_copy(keys_v, keys_out, local.at[12]),
-        pltpu.make_async_copy(values_v, values_out, local.at[13]),
-    ]
-    for each in small:
-        each.start()
 
     gated = TorusGather(
         lambda p: chunk.at[p], gated_all, gat_arrived, gat_first, gat_ring, nz, ny
@@ -497,6 +550,14 @@
     ]
     for each in keep:
         each.start()
+
+    source = iota((4 * seqs, seqs), 0)
+    target = iota((4 * seqs, seqs), 1)
+    for p in range(4):
+        row_seq = 2 * (source >> 3) + ((source >> 1) & 1)
+        row_prop = 2 * ((source >> 2) & 1) + (source & 1)
+        hit = (row_seq == target) & (row_prop == p)
+        order[:, pl.ds(seqs * p, seqs)] = jnp.where(hit, 1.0, 0.0).astype(BF16)
     for k in range(gated.hops()):
         gated.round(k)
     gated.last_arrivals()
@@ -528,9 +589,7 @@
     summed = (sent_out[tp].astype(F32) + got_out[...].astype(F32)).astype(BF16)
     result = jnp.dot(summed, order[...], preferred_element_type=F32).astype(BF16)
     for p in range(4):
-        ret_v[p] = result[:, p * seqs : (p + 1) * seqs]
-    last = pltpu.make_async_copy(ret_v, ret_out, local.at[16])
-    last.start()
+        ret_out[p] = result[:, p * seqs : (p + 1) * seqs]
     tokens.finish()
     gated.finish()
     tokens.loop(1, nz, lambda d: a_copy(d).wait_send())
@@ -541,10 +600,33 @@
 
     tokens.loop(1, ny, b_done)
     b_copy(0, False).wait_send()
-    for each in small:
-        each.wait()
-    state_store.wait()
-    last.wait()
+
+
+def in_hbm(value):
+    return pltpu.with_memory_space_constraint(value, pltpu.HBM)
+
+
+def put_kernel(*refs):
+    count = (len(refs) - 1) // 2
+    sems = refs[-1]
+    copies = [
+        pltpu.make_async_copy(refs[i], refs[count + i], sems.at[i]) for i in range(count)
+    ]
+    for copy in copies:
+        copy.start()
+    for copy in copies:
+        copy.wait()
+
+
+def put_out(*values):
+    return pl.pallas_call(
+        put_kernel,
+        out_shape=tuple(jax.ShapeDtypeStruct(v.shape, v.dtype) for v in values),
+        in_specs=[pl.BlockSpec(memory_space=pl.ANY)] * len(values),
+        out_specs=(pl.BlockSpec(memory_space=pltpu.HBM),) * len(values),
+        scratch_shapes=[pltpu.SemaphoreType.DMA((len(values),))],
+        compiler_params=pltpu.CompilerParams(vmem_limit_bytes=8 * 1024 * 1024),
+    )(*values)
 
 
 def shards(
@@ -569,51 +651,13 @@
     width = norm_gain.shape[0]
     kc, vc = query_weight.shape[1], value_weight.shape[1]
     span = 2 * kc + 2 * vc
-    log_decay = -decay_rate
     count = 8 * heads
-
-    def to_rows(table):
-        table = table.reshape(2, 2, 2, heads, table.shape[-1])
-        return table.transpose(1, 0, 2, 3, 4).reshape(count, -1)
-
     half = key_size // 2
-    steps = jnp.arange(4, dtype=jnp.int32)
-    positions = (lengths + accepted)[:, None] + steps[None, :]
     frequency = jnp.power(10000.0, -jnp.arange(half, dtype=F32) / half)
-    angles = positions.astype(F32)[:, :, None] * frequency
-    cosine, sine = jnp.cos(angles), jnp.sin(angles)
-
-    def all_heads(table):
-        return to_rows(jnp.broadcast_to(table[:, :, None, :], (2, 4, heads, key_size)))
-
-    cos_tab = all_heads(jnp.concatenate([cosine, cosine], axis=-1))
-    sin_tab = all_heads(jnp.concatenate([-sine, sine], axis=-1))
-    row = jnp.arange(count, dtype=jnp.int32)
-    row_prop = 2 * (row // (4 * heads)) + (row // heads) % 2
-    row_seq = (row // (2 * heads)) % 2
-    row_head = row % heads
-    row_decay = jnp.tile(log_decay, 8)
-    offset = (row_prop[:, None] - row_prop[None, :]).astype(F32)
-    same = (row_seq[:, None] == row_seq[None, :]) & (row_head[:, None] == row_head[None, :])
-    grid = jnp.where(
-        same & (offset >= 0.0), jnp.exp(row_decay[:, None] * jnp.maximum(offset, 0.0)), 0.0
-    )
-    query_decay = jnp.broadcast_to(
-        jnp.exp(row_decay * (row_prop.astype(F32) + 1.0))[:, None], (count, key_size)
-    )
-    power = jnp.maximum(accepted[:, None] - 1 - steps[None, :], 0).astype(F32)
-    taken = steps[None, :] < accepted[:, None]
-    weight = jnp.where(
-        taken[:, :, None], jnp.exp(log_decay[None, None, :] * power[:, :, None]), 0.0
-    )
-    key_weights = jnp.broadcast_to(
-        weight.reshape(2, 4 * heads, 1), (2, 4 * heads, key_size)
-    )
-    carried = jnp.exp(log_decay[None, :] * accepted[:, None].astype(F32)).reshape(2 * heads)
-
-    any_ref = pl.BlockSpec(memory_space=pl.ANY)
+    frequency = jnp.concatenate([frequency, frequency])[None, :]
+
+    hbm = pl.BlockSpec(memory_space=pltpu.HBM)
     vmem = pl.BlockSpec(memory_space=pltpu.VMEM)
-    smem = pl.BlockSpec(memory_space=pltpu.SMEM)
     dma = pltpu.SemaphoreType.DMA
     cut = heads * value_size // 2
     out_cols = out_weight.shape[1]
@@ -625,14 +669,19 @@
             jax.ShapeDtypeStruct((2, 4, heads, key_size), BF16),
             jax.ShapeDtypeStruct((2, 4, heads, value_size), BF16),
         ),
-        in_specs=[any_ref] * 7 + [vmem] * 8 + [smem],
-        out_specs=(any_ref,) * 4,
+        in_specs=[hbm] * 12 + [vmem] * 2,
+        out_specs=(vmem,) * 4,
         scratch_shapes=[
             pltpu.VMEM((2, depth, seqs), BF16),
             pltpu.VMEM((2, span, width), BF16),
             pltpu.VMEM((out_cols, heads * value_size), BF16),
             pltpu.VMEM((2 * heads, key_size, value_size), F32),
-            pltpu.VMEM((2 * heads, key_size, value_size), F32),
+            pltpu.VMEM((2, 4 * heads, key_size), BF16),
+            pltpu.VMEM((2, 4 * heads, value_size), BF16),
+            pltpu.SMEM((heads,), F32),
+            pltpu.SMEM((2,), jnp.int32),
+            pltpu.SMEM((2,), jnp.int32),
+            pltpu.VMEM((2, 2, 4 * heads, key_size), F32),
             pltpu.VMEM((2 * heads, key_size, value_size), BF16),
             pltpu.VMEM((2, nz, ny, depth, seqs), BF16),
             pltpu.VMEM((128 * ny, 2 * key_size + 2 * value_size), BF16),
@@ -647,10 +696,7 @@
             pltpu.VMEM((2, nz, ny, 8, cut), BF16),
             pltpu.VMEM((2, out_cols // 2, 4 * seqs), BF16),
             pltpu.VMEM((out_cols // 2, 4 * seqs), BF16),
-            pltpu.VMEM((4, out_cols // 2, seqs), BF16),
-            pltpu.VMEM((2, 4, heads, key_size), BF16),
-            pltpu.VMEM((2, 4, heads, value_size), BF16),
-            dma((17,)),
+            dma((22,)),
             dma((2, nz, ny)),
             dma((2, max(nz, ny))),
             dma((2, 2, nz // 2, ny)),
@@ -667,23 +713,27 @@
             collective_id=0, has_side_effects=True, vmem_limit_bytes=48 * 1024 * 1024
         ),
     )(
-        tokens.transpose(1, 2, 0),
-        query_weight.T,
-        key_weight.T,
-        value_weight.T,
-        gate_weight.T,
-        out_weight.T,
-        prior_state.reshape(2 * heads, key_size, value_size),
+        *map(
+            in_hbm,
+            (
+                tokens.transpose(1, 2, 0),
+                query_weight.T,
+                key_weight.T,
+                value_weight.T,
+                gate_weight.T,
+                out_weight.T,
+                prior_state.reshape(2 * heads, key_size, value_size),
+                last_keys.reshape(2, 4 * heads, key_size),
+                last_values.reshape(2, 4 * heads, value_size),
+                decay_rate,
+                accepted,
+                lengths,
+            ),
+        ),
         norm_gain.astype(F32)[None, :],
-        last_keys.reshape(2, 4 * heads, key_size),
-        last_values.reshape(2, 4 * heads, value_size),
-        cos_tab,
-        sin_tab,
-        grid,
-        query_decay,
-        key_weights,
-        carried,
-    )
+        frequency,
+    )
+    retained, state, new_keys, new_values = put_out(retained, state, new_keys, new_values)
     return (
         retained.transpose(2, 0, 1),
         state.reshape(prior_state.shape),

time: 94.5 us -> 79.1 us (0.84)
  local copies, waits for them, and re-layouts: 12.4 us -> 0 us
  other arithmetic: 3.42 us -> 0.79 us
    unnamed x22 -> x0, local copies, waits for them, and re-layouts: 11.7 us -> none
    pallas_call x0 -> x1, Pallas kernels: none -> 1.37 us  [put_out(): pl.pallas_call(put_kernel, out_shape=tuple((jax.ShapeDtypeStruct(v.shape,...]
    pallas_call x1, Pallas kernels: 77.5 us -> 76.1 us  [shards(): pl.pallas_call(functools.partial(kernel, nz, ny), out_shape=(jax.ShapeDty...]
where the time goes in v2:
time: 79.1 us; the launch traced here: 78.9 us
  Pallas kernels  77.5 us (98%)
    pallas_call x1, Pallas kernels, shards(): pl.pallas_call(functools.partial(kernel, nz, ny), out_shape=(jax.ShapeDty...  76.1 us

profile of v2, /device:TPU:1, one launch (start us, length us, event | category | flops | bytes accessed | tf_op | source)
XLA Modules:
  0.0 78.9 jit_solution(18379778889743126466)
XLA Ops:
  0.6 0.1 maximum_bitcast_fusion.frequency
  0.7 0.7 broadcast_in_dim.11
  1.4 76.1 %shard_map.156 = (bf16[4,32,128]{2,1,0:T(8,128)(2,1)S(1)}, f32[16,128,256]{2,1,0:T(8,128)S(1)}, bf16[2,4,8,128]{3,2,1,0:T(8,128)(2,1)S(1)}, bf16[2,4,8,256]{3,2,1,0:T(8,128)(2,1)S(1)}) custom-call(bf16[4,64,128]{2,1,0:T(8,128)(2,1)} %bitcast.21, bf16[16,4096]{1,0:T(8,128)(2,1)} %bitcast.19, bf16[16,4096]{1,0:T(8,128)(2,1)} %bitcast.20, ...), custom_call_target="tpu_custom_call" | custom-call | tf_op jit(solution)/shard_map/pallas_call | solution.py:664
  77.6 1.4 %shard_map.157 = (bf16[4,32,128]{2,1,0:T(8,128)(2,1)}, f32[16,128,256]{2,1,0:T(8,128)}, bf16[2,4,8,128]{3,2,1,0:T(8,128)(2,1)}, bf16[2,4,8,256]{3,2,1,0:T(8,128)(2,1)}) custom-call(bf16[4,32,128]{2,1,0:T(8,128)(2,1)S(1)} %get-tuple-element.12.refs_0_, f32[16,128,256]{2,1,0:T(8,128)S(1)} %get-tuple-element.13.refs_1_, ...), custom_call_target="tpu_custom_call" | custom-call | tf_op jit(solution)/shard_map/pallas_call | solution.py:622
  (1 shorter events, 0.0 us)

commit v3 on v2

--- a/solution.py
+++ b/solution.py
@@ -22,87 +22,103 @@
     return i & (n - 1)
 
 
-def ring_place(i, n):
-    if isinstance(i, int):
-        return (i + 1) // 2 if i % 2 else (n - i // 2) % n
-    odd = i & 1
-    return wrap(odd * ((i + 1) >> 1) + (1 - odd) * (n - (i >> 1)), n)
+def far_first(i, n):
+    return wrap(n // 2 + (1 - 2 * (i & 1)) * (i >> 1), n)
 
 
 class TorusGather:
-    def __init__(self, own, held, arrived, first_sent, ring_sent, nz, ny):
-        self.own, self.held, self.arrived = own, held, arrived
+    groups = 4
+
+    def __init__(self, own, held, arrived, ring_arrived, first_sent, ring_sent, nz, ny):
+        self.own, self.held, self.arrived, self.ring_arrived = own, held, arrived, ring_arrived
         self.first_sent, self.ring_sent = first_sent, ring_sent
         z, y = lax.axis_index("kv_0"), lax.axis_index("kv_1")
         self.partner = {"tp": 1 - lax.axis_index("tp")}
         self.first = ((y, ny, "kv_1"), (z, nz, "kv_0"))
         self.second = ((z, nz, "kv_0"), (y, ny, "kv_1"))
+        self.hops = nz // 2
+        self.size = ny // self.groups
 
     def at(self, ref, p, f, s):
         return ref.at[p, s, f] if p == 0 else ref.at[p, f, s]
 
-    def copy(self, p, f, s, source, sent, device):
+    def copy(self, target, source, sent, arrived, device):
         return pltpu.make_async_remote_copy(
             src_ref=source,
-            dst_ref=self.at(self.held, p, f, s),
+            dst_ref=target,
             send_sem=sent,
-            recv_sem=self.at(self.arrived, p, f, s),
+            recv_sem=arrived,
             device_id=device,
             device_id_type=MESH,
         )
 
-    def wait(self, p, f, s):
-        chunk = self.at(self.held, p, f, s)
-        self.copy(p, f, s, chunk, self.first_sent.at[0, 0], self.partner).wait_recv()
-
     def first_copy(self, p, d):
         (f, n, axis), (s, _, _) = self.first[p], self.second[p]
         return self.copy(
-            p, f, s, self.own(p), self.first_sent.at[p, d], {axis: wrap(f + d, n)}
+            self.at(self.held, p, f, s),
+            self.own(p),
+            self.first_sent.at[p, d],
+            self.at(self.arrived, p, f, s),
+            {axis: wrap(f + d, n)},
         )
 
     def start_first(self):
+        def send(i):
+            for p in range(2):
+                self.first_copy(p, far_first(i, self.first[p][1])).start()
+
+        self.loop(1, self.first[0][1], send)
         for p in range(2):
-            n = self.first[p][1]
-
-            def send(i, _, p=p, n=n):
-                self.first_copy(p, ring_place(i, n)).start()
-                return 0
-
-            lax.fori_loop(1, n, send, 0)
+            (f, _, _), (s, _, _) = self.first[p], self.second[p]
+            pltpu.make_async_copy(
+                self.own(p), self.at(self.held, p, f, s), self.at(self.arrived, p, f, s)
+            ).start()
+
+    def group(self, p, i):
+        f = self.first[p][0]
+        return wrap(f // self.size + i, self.groups)
+
+    def group_at(self, p, q, s):
+        return self.at(self.held, p, pl.ds(q * self.size, self.size), s)
 
     def ring_copy(self, p, k, i, way):
-        (f, nf, _), (s, ns, axis) = self.first[p], self.second[p]
-        other = wrap(f + ring_place(i, nf), nf)
-        origin = wrap(s - way * k + ns, ns)
-        chunk = self.at(self.held, p, other, origin)
-        if k == 0:
-            source = self.own(p) if isinstance(i, int) and i == 0 else chunk
-        else:
-            source = chunk
-        sent = self.ring_sent.at[p, (1 + way) // 2, k, i]
-        return self.copy(p, other, origin, source, sent, {axis: wrap(s + way + ns, ns)})
+        s, n, axis = self.second[p]
+        q, origin = self.group(p, i), wrap(s - way * k + n, n)
+        block = self.group_at(p, q, origin)
+        return self.copy(
+            block,
+            block,
+            self.ring_sent.at[p, (1 + way) // 2, k, i],
+            self.ring_arrived.at[p, origin, q],
+            {axis: wrap(s + way + n, n)},
+        )
+
+    def wait_chunk(self, p, f, s):
+        chunk = self.at(self.held, p, f, s)
+        self.copy(
+            chunk, chunk, self.first_sent.at[0, 0], self.at(self.arrived, p, f, s), self.partner
+        ).wait_recv()
+
+    def wait_group(self, p, i, s):
+        q = self.group(p, i)
+        block = self.group_at(p, q, s)
+        self.copy(
+            block, block, self.first_sent.at[0, 0], self.ring_arrived.at[p, s, q], self.partner
+        ).wait_recv()
 
     def pass_on(self, k, i, ways):
         for p in range(2):
-            (f, nf, _), (s, ns, _) = self.first[p], self.second[p]
-            other = wrap(f + ring_place(i, nf), nf)
+            s, n, _ = self.second[p]
             if k == 0:
-                if not (isinstance(i, int) and i == 0):
-                    self.wait(p, other, s)
+                for e in range(self.size):
+                    self.wait_chunk(p, self.group(p, i) * self.size + e, s)
                 for way in ways:
                     self.ring_copy(p, k, i, way).start()
             else:
                 for way in (1, -1):
-                    self.wait(p, other, wrap(s - way * k + ns, ns))
+                    self.wait_group(p, i, wrap(s - way * k + n, n))
                     if way in ways:
                         self.ring_copy(p, k, i, way).start()
-
-    def hops(self):
-        return self.second[0][1] // 2
-
-    def start_ring(self):
-        self.pass_on(0, 0, (1, -1))
 
     def loop(self, low, high, step):
         def body(i, _):
@@ -111,47 +127,43 @@
 
         lax.fori_loop(low, high, body, 0)
 
+    def over_groups(self, k, step):
+        if k < self.hops - 1:
+            self.loop(0, self.groups, lambda i: step(i, (1, -1)))
+        else:
+            self.loop(0, self.groups // 2, lambda i: step(i, (1,)))
+            self.loop(self.groups // 2, self.groups, lambda i: step(i, (-1,)))
+
     def round(self, k, beside=None):
-        n = self.first[0][1]
-
-        def both(i, ways):
+        def step(i, ways):
             self.pass_on(k, i, ways)
             if beside is not None:
                 beside(i)
 
-        if k < self.hops() - 1:
-            self.loop(1 if k == 0 else 0, n, lambda i: both(i, (1, -1)))
-        else:
-            self.loop(0, n // 2, lambda i: both(i, (1,)))
-            self.loop(n // 2, n, lambda i: both(i, (-1,)))
+        self.over_groups(k, step)
 
     def last_arrivals(self):
-        k = self.hops()
-
         def take(i):
             for p in range(2):
-                (f, nf, _), (s, ns, _) = self.first[p], self.second[p]
-                self.wait(p, wrap(f + ring_place(i, nf), nf), wrap(s + k, ns))
-
-        self.loop(0, self.first[0][1], take)
+                s, n, _ = self.second[p]
+                self.wait_group(p, i, wrap(s + self.hops, n))
+
+        self.loop(0, self.groups, take)
 
     def finish(self):
-        n = self.first[0][1]
-        for p in range(2):
-            self.loop(1, n, lambda d, p=p: self.first_copy(p, d).wait_send())
-        for k in range(self.hops()):
-            last = k == self.hops() - 1
+        def first_done(d):
+            for p in range(2):
+                self.first_copy(p, d).wait_send()
+
+        self.loop(1, self.first[0][1], first_done)
+        for k in range(self.hops):
 
             def done(i, ways, k=k):
                 for p in range(2):
                     for way in ways:
                         self.ring_copy(p, k, i, way).wait_send()
 
-            if last:
-                self.loop(0, n // 2, lambda i: done(i, (1,)))
-                self.loop(n // 2, n, lambda i: done(i, (-1,)))
-            else:
-                self.loop(0, n, lambda i: done(i, (1, -1)))
+            self.over_groups(k, done)
 
 
 def iota(shape, dim):
@@ -205,9 +217,11 @@
     got_out,
     local,
     tok_arrived,
+    tok_passed,
     tok_first,
     tok_ring,
     gat_arrived,
+    gat_passed,
     gat_first,
     gat_ring,
     pair_sems,
@@ -269,15 +283,9 @@
 
     loads[0].wait()
     tokens = TorusGather(
-        lambda p: tok_v.at[p], tokens_all, tok_arrived, tok_first, tok_ring, nz, ny
+        lambda p: tok_v.at[p], tokens_all, tok_arrived, tok_passed, tok_first, tok_ring, nz, ny
     )
     tokens.start_first()
-    tokens.start_ring()
-    keep = [
-        pltpu.make_async_copy(tok_v.at[p], tokens_all.at[p, z, y], local.at[7 + p]) for p in range(2)
-    ]
-    for each in keep:
-        each.start()
     for load in loads[1:5]:
         load.wait()
     swap = pltpu.make_async_remote_copy(
@@ -331,25 +339,26 @@
             state_out[at] = fresh
             state_b[at] = fresh.astype(BF16)
 
-    one_head(0)
-    tokens.round(0, one_head)
+    def some_heads(i):
+        for e in range(heads // tokens.groups):
+            one_head(i * (heads // tokens.groups) + e)
+
+    tokens.round(0, some_heads)
 
     swap.wait()
 
     blocks = span // 16
 
     def scale_rows(i):
-        @pl.when(i < blocks)
-        def _():
-            at = pl.ds(pl.multiple_of(i * 16, 16), 16)
-            for side in range(2):
-                weights[side, at] = (weights[side, at].astype(F32) * gain[...]).astype(BF16)
-
-    for k in range(1, tokens.hops()):
-        tokens.round(k, scale_rows if k == 1 else None)
+        at = pl.ds(pl.multiple_of(i * 16, 16), 16)
+        for side in range(2):
+            weights[side, at] = (weights[side, at].astype(F32) * gain[...]).astype(BF16)
+
+    for k in range(1, tokens.hops):
+        tokens.round(k, scale_rows if k < tokens.hops - 1 else None)
+        if k == 1:
+            scale_rows = lambda i, first=scale_rows: pl.when(i + 4 < blocks)(lambda: first(i + 4))
     tokens.last_arrivals()
-    for each in keep:
-        each.wait()
 
     depth = tok_v.shape[1]
     width = nz * ny * depth
@@ -395,7 +404,7 @@
             device_id_type=MESH,
         ).wait_recv()
 
-    tokens.loop(1, nz, lambda d: a_copy(d).start())
+    tokens.loop(1, nz, lambda i: a_copy(far_first(i, nz)).start())
     own_a = pltpu.make_async_copy(out_a.at[z], in_a.at[z], local.at[10])
     own_a.start()
 
@@ -462,7 +471,8 @@
             device_id_type=MESH,
         ).wait_recv()
 
-    def b_start(d):
+    def b_start(i):
+        d = far_first(i, ny)
         b_copy(d, True).start()
         b_copy(d, False).start()
 
@@ -541,16 +551,9 @@
             chunk[part, :, at + 128 * c : at + 128 * (c + 1)] = piece.astype(BF16)
 
     gated = TorusGather(
-        lambda p: chunk.at[p], gated_all, gat_arrived, gat_first, gat_ring, nz, ny
+        lambda p: chunk.at[p], gated_all, gat_arrived, gat_passed, gat_first, gat_ring, nz, ny
     )
     gated.start_first()
-    gated.start_ring()
-    keep = [
-        pltpu.make_async_copy(chunk.at[p], gated_all.at[p, z, y], local.at[14 + p]) for p in range(2)
-    ]
-    for each in keep:
-        each.start()
-
     source = iota((4 * seqs, seqs), 0)
     target = iota((4 * seqs, seqs), 1)
     for p in range(4):
@@ -558,11 +561,9 @@
         row_prop = 2 * ((source >> 2) & 1) + (source & 1)
         hit = (row_seq == target) & (row_prop == p)
         order[:, pl.ds(seqs * p, seqs)] = jnp.where(hit, 1.0, 0.0).astype(BF16)
-    for k in range(gated.hops()):
+    for k in range(gated.hops):
         gated.round(k)
     gated.last_arrivals()
-    for each in keep:
-        each.wait()
     loads[6].wait()
     total = jnp.zeros((wo_v.shape[0], 4 * seqs), F32)
     for part in range(2):
@@ -698,11 +699,13 @@
             pltpu.VMEM((out_cols // 2, 4 * seqs), BF16),
             dma((22,)),
             dma((2, nz, ny)),
+            dma((2, max(nz, ny), TorusGather.groups)),
             dma((2, max(nz, ny))),
-            dma((2, 2, nz // 2, ny)),
+            dma((2, 2, nz // 2, TorusGather.groups)),
             dma((2, nz, ny)),
+            dma((2, max(nz, ny), TorusGather.groups)),
             dma((2, max(nz, ny))),
-            dma((2, 2, nz // 2, ny)),
+            dma((2, 2, nz // 2, TorusGather.groups)),
             dma((4,)),
             dma((nz,)),
             dma((nz,)),

time: 79.1 us -> 79.1 us (level)
  no operation moved by 1% of the time
where the time goes in v3:
time: 79.1 us; the launch traced here: 78.9 us
  Pallas kernels  77.5 us (98%)
    pallas_call x1, Pallas kernels, shards(): pl.pallas_call(functools.partial(kernel, nz, ny), out_shape=(jax.ShapeDty...  76.1 us

profile of v3, /device:TPU:1, one launch (start us, length us, event | category | flops | bytes accessed | tf_op | source)
XLA Modules:
  0.0 78.9 jit_solution(14701612192665214786)
XLA Ops:
  0.6 0.1 maximum_bitcast_fusion.frequency
  0.7 0.7 broadcast_in_dim.11
  1.4 76.1 %shard_map.156 = (bf16[4,32,128]{2,1,0:T(8,128)(2,1)S(1)}, f32[16,128,256]{2,1,0:T(8,128)S(1)}, bf16[2,4,8,128]{3,2,1,0:T(8,128)(2,1)S(1)}, bf16[2,4,8,256]{3,2,1,0:T(8,128)(2,1)S(1)}) custom-call(bf16[4,64,128]{2,1,0:T(8,128)(2,1)} %bitcast.21, bf16[16,4096]{1,0:T(8,128)(2,1)} %bitcast.19, bf16[16,4096]{1,0:T(8,128)(2,1)} %bitcast.20, ...), custom_call_target="tpu_custom_call" | custom-call | tf_op jit(solution)/shard_map/pallas_call | solution.py:665
  77.5 1.4 %shard_map.157 = (bf16[4,32,128]{2,1,0:T(8,128)(2,1)}, f32[16,128,256]{2,1,0:T(8,128)}, bf16[2,4,8,128]{3,2,1,0:T(8,128)(2,1)}, bf16[2,4,8,256]{3,2,1,0:T(8,128)(2,1)}) custom-call(bf16[4,32,128]{2,1,0:T(8,128)(2,1)S(1)} %get-tuple-element.12.refs_0_, f32[16,128,256]{2,1,0:T(8,128)S(1)} %get-tuple-element.13.refs_1_, ...), custom_call_target="tpu_custom_call" | custom-call | tf_op jit(solution)/shard_map/pallas_call | solution.py:623
  (1 shorter events, 0.0 us)

commit v4 on v3

--- a/solution.py
+++ b/solution.py
@@ -166,11 +166,133 @@
             self.over_groups(k, done)
 
 
+class WeightRing:
+    def __init__(self, held, arrived, sent, side_arrived, side_sent, on_arrived, on_sent, nx, nz, ny):
+        self.held, self.arrived, self.sent = held, arrived, sent
+        self.side_arrived, self.side_sent = side_arrived, side_sent
+        self.on_arrived, self.on_sent = on_arrived, on_sent
+        self.x, self.nx = lax.axis_index("dp"), nx
+        z, y = lax.axis_index("kv_0"), lax.axis_index("kv_1")
+        self.partner = {"tp": 1 - lax.axis_index("tp")}
+        self.second = ((z, nz, "kv_0"), (y, ny, "kv_1"))
+        self.hops = nz // 2
+        self.rows = held.shape[2] // nx
+
+    def block(self, p, origin, x):
+        return self.held.at[p, origin, pl.ds(pl.multiple_of(self.rows * x, self.rows), self.rows)]
+
+    def copy(self, block, sent, arrived, device):
+        return pltpu.make_async_remote_copy(
+            src_ref=block,
+            dst_ref=block,
+            send_sem=sent,
+            recv_sem=arrived,
+            device_id=device,
+            device_id_type=MESH,
+        )
+
+    def ring_copy(self, p, k, way):
+        s, n, axis = self.second[p]
+        origin = wrap(s - way * k + n, n)
+        return self.copy(
+            self.block(p, origin, self.x),
+            self.sent.at[p, (1 + way) // 2, k],
+            self.arrived.at[p, origin],
+            {axis: wrap(s + way + n, n)},
+        )
+
+    def side_copy(self, p, origin, way):
+        at = (1 + way) // 2
+        return self.copy(
+            self.block(p, origin, self.x),
+            self.side_sent.at[p, at, origin],
+            self.side_arrived.at[p, at, origin],
+            {"dp": wrap(self.x + way + self.nx, self.nx)},
+        )
+
+    def on_way(self, p):
+        return 1 - 2 * p
+
+    def on_copy(self, p):
+        way = self.on_way(p)
+        x = wrap(self.x - way + self.nx, self.nx)
+        block = self.held.at[p, :, pl.ds(pl.multiple_of(self.rows * x, self.rows), self.rows)]
+        return self.copy(
+            block,
+            self.on_sent.at[p],
+            self.on_arrived.at[p],
+            {"dp": wrap(self.x + way + self.nx, self.nx)},
+        )
+
+    def forward_ways(self, p, k):
+        if k < self.hops - 1:
+            return (1, -1)
+        return (self.on_way(p),) if k == self.hops - 1 else ()
+
+    def step(self, k):
+        for p in range(2):
+            s, n, _ = self.second[p]
+            for way in (1,) if k in (0, self.hops) else (1, -1):
+                origin = wrap(s - way * k + n, n)
+                if k > 0:
+                    self.copy(
+                        self.block(p, origin, self.x),
+                        self.sent.at[0, 0, 0],
+                        self.arrived.at[p, origin],
+                        self.partner,
+                    ).wait_recv()
+                ways = self.forward_ways(p, k)
+                for to in ways if k == 0 else (way,):
+                    if to in ways:
+                        self.ring_copy(p, k, to).start()
+                for to in (1, -1):
+                    self.side_copy(p, origin, to).start()
+
+    def side_wait(self, p, way):
+        x = wrap(self.x - way + self.nx, self.nx)
+
+        def take(origin, _):
+            self.copy(
+                self.block(p, origin, x),
+                self.sent.at[0, 0, 0],
+                self.side_arrived.at[p, (1 + way) // 2, origin],
+                self.partner,
+            ).wait_recv()
+            return 0
+
+        lax.fori_loop(0, self.second[p][1], take, 0)
+
+    def share_on(self):
+        for p in range(2):
+            self.side_wait(p, self.on_way(p))
+            self.on_copy(p).start()
+
+    def all_here(self):
+        for p in range(2):
+            self.side_wait(p, -self.on_way(p))
+            self.on_copy(p).wait_recv()
+
+    def finish(self):
+        for p in range(2):
+            for k in range(self.hops):
+                for way in self.forward_ways(p, k):
+                    self.ring_copy(p, k, way).wait_send()
+
+            def done(origin, _, p=p):
+                for way in (1, -1):
+                    self.side_copy(p, origin, way).wait_send()
+                return 0
+
+            lax.fori_loop(0, self.second[p][1], done, 0)
+            self.on_copy(p).wait_send()
+
+
 def iota(shape, dim):
     return lax.broadcasted_iota(jnp.int32, shape, dim)
 
 
 def kernel(
+    nx,
     nz,
     ny,
     tok,
@@ -193,7 +315,7 @@
     values_out,
     tok_v,
     weights,
-    wo_v,
+    wo_all,
     prior_v,
     last_k,
     last_v,
@@ -213,24 +335,30 @@
     rows_f,
     chunk,
     gated_all,
-    sent_out,
-    got_out,
+    out_c,
+    in_c,
     local,
     tok_arrived,
     tok_passed,
     tok_first,
     tok_ring,
-    gat_arrived,
-    gat_passed,
-    gat_first,
-    gat_ring,
+    wo_arrived,
+    wo_sent,
+    wo_side,
+    wo_side_sent,
+    wo_on,
+    wo_on_sent,
+    g_sent,
+    g_got,
+    c_sent,
+    c_got,
     pair_sems,
     a_sent,
     a_got,
     b_sent,
     b_got,
 ):
-    z, y, tp = lax.axis_index("kv_0"), lax.axis_index("kv_1"), lax.axis_index("tp")
+    x, z, y, tp = (lax.axis_index(axis) for axis in ("dp", "kv_0", "kv_1", "tp"))
     heads, seqs = nz, 2 * nz * ny
     kc = wq.shape[0]
     vc = wv.shape[0]
@@ -244,7 +372,6 @@
         pltpu.make_async_copy(wv, weights.at[tp, pl.ds(2 * kc, vc)], local.at[3]),
         pltpu.make_async_copy(wg, weights.at[tp, pl.ds(2 * kc + vc, vc)], local.at[4]),
         pltpu.make_async_copy(prior, prior_v, local.at[5]),
-        pltpu.make_async_copy(wo, wo_v, local.at[6]),
     ]
     small_loads = [
         pltpu.make_async_copy(source, target, local.at[17 + i])
@@ -258,7 +385,16 @@
             )
         )
     ]
-    for load in loads + small_loads:
+    share = wo.shape[0] // nx
+    mine = pl.ds(pl.multiple_of(share * x, share), share)
+    half_k = wo.shape[1] // 2
+    own_out = [
+        pltpu.make_async_copy(
+            wo.at[mine, pl.ds(p * half_k, half_k)], wo_all.at[p, (z, y)[p], mine], local.at[7 + p]
+        )
+        for p in range(2)
+    ]
+    for load in loads + own_out + small_loads:
         load.start()
 
     barrier = pltpu.get_barrier_semaphore()
@@ -278,14 +414,27 @@
 
     lax.fori_loop(1, ny, greet_y, 0)
     lax.fori_loop(1, nz, greet_z, 0)
+    def greet_tall(d, _):
+        greet({"kv_0": wrap(z + d, nz), "tp": 1 - tp})
+        return 0
+
+    lax.fori_loop(1, nz, greet_tall, 0)
     greet(partner)
-    pl.semaphore_wait(barrier, 2 * (ny - 1) + (nz - 1) + 1)
+    for way in (1, nx - 1):
+        greet({"dp": wrap(x + way, nx)})
+    pl.semaphore_wait(barrier, 2 * (ny - 1) + 2 * (nz - 1) + 3)
 
     loads[0].wait()
     tokens = TorusGather(
         lambda p: tok_v.at[p], tokens_all, tok_arrived, tok_passed, tok_first, tok_ring, nz, ny
     )
     tokens.start_first()
+    ring = WeightRing(
+        wo_all, wo_arrived, wo_sent, wo_side, wo_side_sent, wo_on, wo_on_sent, nx, nz, ny
+    )
+    for load in own_out:
+        load.wait()
+    ring.step(0)
     for load in loads[1:5]:
         load.wait()
     swap = pltpu.make_async_remote_copy(
@@ -355,9 +504,11 @@
             weights[side, at] = (weights[side, at].astype(F32) * gain[...]).astype(BF16)
 
     for k in range(1, tokens.hops):
+        ring.step(k)
         tokens.round(k, scale_rows if k < tokens.hops - 1 else None)
         if k == 1:
             scale_rows = lambda i, first=scale_rows: pl.when(i + 4 < blocks)(lambda: first(i + 4))
+    ring.step(tokens.hops)
     tokens.last_arrivals()
 
     depth = tok_v.shape[1]
@@ -407,6 +558,7 @@
     tokens.loop(1, nz, lambda i: a_copy(far_first(i, nz)).start())
     own_a = pltpu.make_async_copy(out_a.at[z], in_a.at[z], local.at[10])
     own_a.start()
+    ring.share_on()
 
     shift = heads.bit_length() - 1
 
@@ -550,49 +702,129 @@
             piece = rows_f[c, pl.ds(h, 8, stride=heads), :]
             chunk[part, :, at + 128 * c : at + 128 * (c + 1)] = piece.astype(BF16)
 
-    gated = TorusGather(
-        lambda p: chunk.at[p], gated_all, gat_arrived, gat_passed, gat_first, gat_ring, nz, ny
-    )
-    gated.start_first()
+    first = ((y, ny, "kv_1"), (z, nz, "kv_0"))
+    second = ((z, nz, "kv_0"), (y, ny, "kv_1"))
+
+    def g_copy(p, d):
+        f, n, axis = first[p]
+        return pltpu.make_async_remote_copy(
+            src_ref=chunk.at[p],
+            dst_ref=gated_all.at[p, f],
+            send_sem=g_sent.at[p, d],
+            recv_sem=g_got.at[p, f],
+            device_id={axis: wrap(f + d, n)},
+            device_id_type=MESH,
+        )
+
+    def g_start(i):
+        for p in range(2):
+            g_copy(p, far_first(i, first[p][1])).start()
+
+    tokens.loop(1, ny, g_start)
+    for p in range(2):
+        f = first[p][0]
+        pltpu.make_async_copy(chunk.at[p], gated_all.at[p, f], g_got.at[p, f]).start()
+
     source = iota((4 * seqs, seqs), 0)
     target = iota((4 * seqs, seqs), 1)
-    for p in range(4):
-        row_seq = 2 * (source >> 3) + ((source >> 1) & 1)
+    low_ring, high_ring = (source >> 3) & (ny - 1), source >> (2 + ny.bit_length())
+    for part, group in enumerate((high_ring * ny + low_ring, low_ring * ny + high_ring)):
+        row_seq = 2 * group + ((source >> 1) & 1)
         row_prop = 2 * ((source >> 2) & 1) + (source & 1)
-        hit = (row_seq == target) & (row_prop == p)
-        order[:, pl.ds(seqs * p, seqs)] = jnp.where(hit, 1.0, 0.0).astype(BF16)
-    for k in range(gated.hops):
-        gated.round(k)
-    gated.last_arrivals()
-    loads[6].wait()
-    total = jnp.zeros((wo_v.shape[0], 4 * seqs), F32)
-    for part in range(2):
-        total += lax.dot_general(
-            wo_v[:, part * cut : (part + 1) * cut],
-            gated_all[part].reshape(4 * seqs, cut),
+        for p in range(4):
+            hit = (row_seq == target) & (row_prop == p)
+            order[part, :, pl.ds(seqs * p, seqs)] = jnp.where(hit, 1.0, 0.0).astype(BF16)
+    ring.all_here()
+
+    def c_copy(p, d, same):
+        s, n, axis = second[p]
+        to = wrap(s + d, n)
+        side = tp if same else 1 - tp
+        return pltpu.make_async_remote_copy(
+            src_ref=out_c.at[p, to, side],
+            dst_ref=in_c.at[p, tp, s],
+            send_sem=c_sent.at[p, d, side],
+            recv_sem=c_got.at[p, tp, s],
+            device_id={axis: to, "tp": side},
+            device_id_type=MESH,
+        )
+
+    def wait_for(block, arrived):
+        pltpu.make_async_remote_copy(
+            src_ref=block,
+            dst_ref=block,
+            send_sem=a_sent.at[0],
+            recv_sem=arrived,
+            device_id=partner,
+            device_id_type=MESH,
+        ).wait_recv()
+
+    out_cols = wo.shape[0]
+    for p in range(2):
+        n = first[p][1]
+        tokens.loop(0, n, lambda f, p=p: wait_for(gated_all.at[p, f], g_got.at[p, f]))
+        product = lax.dot_general(
+            wo_all[p].reshape(second[p][1] * out_cols, cut),
+            gated_all[p].reshape(n * 8, cut),
             (((1,), (1,)), ((), ())),
             preferred_element_type=F32,
         )
-    rounded = total.astype(BF16)
-    mine = rounded.shape[0] // 2
-    sent_out[0] = rounded[:mine]
-    sent_out[1] = rounded[mine:]
-    trade = pltpu.make_async_remote_copy(
-        src_ref=sent_out.at[1 - tp],
-        dst_ref=got_out,
-        send_sem=pair_sems.at[2],
-        recv_sem=pair_sems.at[3],
-        device_id=partner,
-        device_id_type=MESH,
-    )
-    trade.start()
-    trade.wait()
-    summed = (sent_out[tp].astype(F32) + got_out[...].astype(F32)).astype(BF16)
-    result = jnp.dot(summed, order[...], preferred_element_type=F32).astype(BF16)
+        blank = jnp.zeros_like(product)
+        lanes = jnp.where(
+            (second[p][0] & 1) == 0,
+            jnp.concatenate([product, blank], axis=1),
+            jnp.concatenate([blank, product], axis=1),
+        ).astype(BF16)
+        part = out_cols // 2
+        for to in range(second[p][1]):
+            for side in range(2):
+                at = to * out_cols + side * part
+                out_c[p, to, side] = lanes[at : at + part]
+
+        def c_start(i, p=p, n=n):
+            d = far_first(i, n)
+            c_copy(p, d, True).start()
+            c_copy(p, d, False).start()
+
+        tokens.loop(1, n, c_start)
+        c_copy(p, 0, False).start()
+        s = second[p][0]
+        pltpu.make_async_copy(
+            out_c.at[p, s, tp], in_c.at[p, tp, s], c_got.at[p, tp, s]
+        ).start()
+    result = jnp.zeros((out_cols // 2, 4 * seqs), F32)
+    for p in range(2):
+        n = second[p][1]
+        for side in range(2):
+            tokens.loop(
+                0, n, lambda s, p=p, side=side: wait_for(in_c.at[p, side, s], c_got.at[p, side, s])
+            )
+        sums = jnp.concatenate(
+            [
+                jnp.concatenate(
+                    [in_c[p, side, 2 * j] + in_c[p, side, 2 * j + 1] for j in range(n // 2)], axis=1
+                )
+                for side in range(2)
+            ],
+            axis=0,
+        )
+        moved = jnp.dot(sums, order[p], preferred_element_type=F32)
+        result += moved[: out_cols // 2] + moved[out_cols // 2 :]
+    result = result.astype(BF16)
     for p in range(4):
         ret_out[p] = result[:, p * seqs : (p + 1) * seqs]
     tokens.finish()
-    gated.finish()
+    ring.finish()
+
+    def late_done(d):
+        for p in range(2):
+            g_copy(p, d).wait_send()
+            for same in (True, False):
+                c_copy(p, d, same).wait_send()
+
+    tokens.loop(1, ny, late_done)
+    for p in range(2):
+        c_copy(p, 0, False).wait_send()
     tokens.loop(1, nz, lambda d: a_copy(d).wait_send())
 
     def b_done(d):
@@ -631,6 +863,7 @@
 
 
 def shards(
+    nx,
     nz,
     ny,
     tokens,
@@ -663,7 +896,7 @@
     cut = heads * value_size // 2
     out_cols = out_weight.shape[1]
     retained, state, new_keys, new_values = pl.pallas_call(
-        functools.partial(kernel, nz, ny),
+        functools.partial(kernel, nx, nz, ny),
         out_shape=(
             jax.ShapeDtypeStruct((4, out_cols // 2, seqs), BF16),
             jax.ShapeDtypeStruct((2 * heads, key_size, value_size), F32),
@@ -675,7 +908,7 @@
         scratch_shapes=[
             pltpu.VMEM((2, depth, seqs), BF16),
             pltpu.VMEM((2, span, width), BF16),
-            pltpu.VMEM((out_cols, heads * value_size), BF16),
+            pltpu.VMEM((2, nz, out_cols, cut), BF16),
             pltpu.VMEM((2 * heads, key_size, value_size), F32),
             pltpu.VMEM((2, 4 * heads, key_size), BF16),
             pltpu.VMEM((2, 4 * heads, value_size), BF16),
@@ -686,7 +919,7 @@
             pltpu.VMEM((2 * heads, key_size, value_size), BF16),
             pltpu.VMEM((2, nz, ny, depth, seqs), BF16),
             pltpu.VMEM((128 * ny, 2 * key_size + 2 * value_size), BF16),
-            pltpu.VMEM((4 * seqs, 4 * seqs), BF16),
+            pltpu.VMEM((2, 4 * seqs, 4 * seqs), BF16),
             pltpu.VMEM((nz, 2, 2, 2 * ny, 128), BF16),
             pltpu.VMEM((nz, 2, 2, 2 * ny, 128), BF16),
             pltpu.VMEM((nz * 8 * ny, 128), F32),
@@ -694,18 +927,24 @@
             pltpu.VMEM((ny, 2, 2, 2 * nz, 128), BF16),
             pltpu.VMEM((value_size // 128, count, 128), F32),
             pltpu.VMEM((2, 8, cut), BF16),
-            pltpu.VMEM((2, nz, ny, 8, cut), BF16),
-            pltpu.VMEM((2, out_cols // 2, 4 * seqs), BF16),
-            pltpu.VMEM((out_cols // 2, 4 * seqs), BF16),
+            pltpu.VMEM((2, nz, 8, cut), BF16),
+            pltpu.VMEM((2, nz, 2, out_cols // 2, 128), BF16),
+            pltpu.VMEM((2, 2, nz, out_cols // 2, 128), BF16),
             dma((22,)),
             dma((2, nz, ny)),
             dma((2, max(nz, ny), TorusGather.groups)),
             dma((2, max(nz, ny))),
             dma((2, 2, nz // 2, TorusGather.groups)),
-            dma((2, nz, ny)),
-            dma((2, max(nz, ny), TorusGather.groups)),
-            dma((2, max(nz, ny))),
-            dma((2, 2, nz // 2, TorusGather.groups)),
+            dma((2, nz)),
+            dma((2, 2, nz // 2)),
+            dma((2, 2, nz)),
+            dma((2, 2, nz)),
+            dma((2,)),
+            dma((2,)),
+            dma((2, nz)),
+            dma((2, nz)),
+            dma((2, nz, 2)),
+            dma((2, 2, nz)),
             dma((4,)),
             dma((nz,)),
             dma((nz,)),
@@ -752,7 +991,7 @@
         ("dp", "kv_0", "kv_1", "tp"),
     )
     return jax.shard_map(
-        functools.partial(shards, nz, ny),
+        functools.partial(shards, mesh.shape["dp"], nz, ny),
         mesh=finer,
         in_specs=(
             P("dp", None, KV),

time: 79.1 us -> 69.2 us (0.87)
  Pallas kernels: 77.5 us -> 67.6 us
    pallas_call x1, Pallas kernels: 76.1 us -> 66.2 us  [shards(): pl.pallas_call(functools.partial(kernel, nx, nz, ny), out_shape=(jax.Shap...]
where the time goes in v4:
time: 69.2 us; the launch traced here: 69 us
  Pallas kernels  67.6 us (98%)
  other arithmetic  0.79 us (1%)
    pallas_call x1, Pallas kernels, shards(): pl.pallas_call(functools.partial(kernel, nx, nz, ny), out_shape=(jax.Shap...  66.2 us

profile of v4, /device:TPU:1, one launch (start us, length us, event | category | flops | bytes accessed | tf_op | source)
XLA Modules:
  0.0 69.0 jit_solution(18133678938034468733)
XLA Ops:
  0.6 0.1 maximum_bitcast_fusion.frequency
  0.7 0.7 %broadcast_in_dim.11 = f32[4096]{0:T(1024)S(1)} convert(bf16[4096]{0:T(1024)(128)(2,1)} %param.14) | non-fusion elementwise | flops 4096 | bytes 24576 | tf_op jit(solution)/shard_map/broadcast_in_dim | solution.py:975
  1.4 66.2 %shard_map.156 = (bf16[4,32,128]{2,1,0:T(8,128)(2,1)S(1)}, f32[16,128,256]{2,1,0:T(8,128)S(1)}, bf16[2,4,8,128]{3,2,1,0:T(8,128)(2,1)S(1)}, bf16[2,4,8,256]{3,2,1,0:T(8,128)(2,1)S(1)}) custom-call(bf16[4,64,128]{2,1,0:T(8,128)(2,1)} %bitcast.21, bf16[16,4096]{1,0:T(8,128)(2,1)} %bitcast.19, bf16[16,4096]{1,0:T(8,128)(2,1)} %bitcast.20, ...), custom_call_target="tpu_custom_call" | custom-call | tf_op jit(solution)/shard_map/pallas_call | solution.py:898
  67.6 1.4 %shard_map.157 = (bf16[4,32,128]{2,1,0:T(8,128)(2,1)}, f32[16,128,256]{2,1,0:T(8,128)}, bf16[2,4,8,128]{3,2,1,0:T(8,128)(2,1)}, bf16[2,4,8,256]{3,2,1,0:T(8,128)(2,1)}) custom-call(bf16[4,32,128]{2,1,0:T(8,128)(2,1)S(1)} %get-tuple-element.12.refs_0_, f32[16,128,256]{2,1,0:T(8,128)S(1)} %get-tuple-element.13.refs_1_, ...), custom_call_target="tpu_custom_call" | custom-call | tf_op jit(solution)/shard_map/pallas_call | solution.py:855
  (1 shorter events, 0.0 us)

commit v5 on v4

--- a/solution.py
+++ b/solution.py
@@ -26,8 +26,14 @@
     return wrap(n // 2 + (1 - 2 * (i & 1)) * (i >> 1), n)
 
 
+def near_first(i, n):
+    odd = i & 1
+    return wrap(odd * ((i + 1) >> 1) + (1 - odd) * (n - (i >> 1)), n)
+
+
 class TorusGather:
     groups = 4
+    turn = (0, 1, 3, 2)
 
     def __init__(self, own, held, arrived, ring_arrived, first_sent, ring_sent, nz, ny):
         self.own, self.held, self.arrived, self.ring_arrived = own, held, arrived, ring_arrived
@@ -65,7 +71,7 @@
     def start_first(self):
         def send(i):
             for p in range(2):
-                self.first_copy(p, far_first(i, self.first[p][1])).start()
+                self.first_copy(p, near_first(i, self.first[p][1])).start()
 
         self.loop(1, self.first[0][1], send)
         for p in range(2):
@@ -76,7 +82,7 @@
 
     def group(self, p, i):
         f = self.first[p][0]
-        return wrap(f // self.size + i, self.groups)
+        return wrap(f // self.size + self.turn[i], self.groups)
 
     def group_at(self, p, q, s):
         return self.at(self.held, p, pl.ds(q * self.size, self.size), s)
@@ -127,28 +133,27 @@
 
         lax.fori_loop(low, high, body, 0)
 
-    def over_groups(self, k, step):
+    def ways(self, k, i):
         if k < self.hops - 1:
-            self.loop(0, self.groups, lambda i: step(i, (1, -1)))
-        else:
-            self.loop(0, self.groups // 2, lambda i: step(i, (1,)))
-            self.loop(self.groups // 2, self.groups, lambda i: step(i, (-1,)))
-
-    def round(self, k, beside=None):
-        def step(i, ways):
-            self.pass_on(k, i, ways)
-            if beside is not None:
-                beside(i)
-
-        self.over_groups(k, step)
+            return (1, -1)
+        return (1,) if i < self.groups // 2 else (-1,)
+
+    def wave(self, w, beside=None):
+        for k in reversed(range(self.hops)):
+            i = w - k
+            if 0 <= i < self.groups:
+                self.pass_on(k, i, self.ways(k, i))
+                if beside is not None:
+                    beside()
+
+    def waves(self):
+        return self.hops + self.groups - 1
 
     def last_arrivals(self):
-        def take(i):
+        for i in range(self.groups):
             for p in range(2):
                 s, n, _ = self.second[p]
                 self.wait_group(p, i, wrap(s + self.hops, n))
-
-        self.loop(0, self.groups, take)
 
     def finish(self):
         def first_done(d):
@@ -157,13 +162,10 @@
 
         self.loop(1, self.first[0][1], first_done)
         for k in range(self.hops):
-
-            def done(i, ways, k=k):
+            for i in range(self.groups):
                 for p in range(2):
-                    for way in ways:
+                    for way in self.ways(k, i):
                         self.ring_copy(p, k, i, way).wait_send()
-
-            self.over_groups(k, done)
 
 
 class WeightRing:
@@ -307,7 +309,7 @@
     decay_in,
     accepted_in,
     lengths_in,
-    gain,
+    gain_in,
     frequency,
     ret_out,
     state_out,
@@ -322,6 +324,8 @@
     decay,
     accepted,
     lengths,
+    gain_v,
+    gain,
     weighted_keys,
     state_b,
     tokens_all,
@@ -363,6 +367,8 @@
     kc = wq.shape[0]
     vc = wv.shape[0]
     span = 2 * kc + 2 * vc
+    depth = tok_v.shape[1]
+    width = nz * ny * depth
     partner = {"tp": 1 - tp}
 
     loads = [
@@ -382,6 +388,7 @@
                 (decay_in, decay),
                 (accepted_in, accepted),
                 (lengths_in, lengths),
+                (gain_in, gain_v),
             )
         )
     ]
@@ -488,31 +495,35 @@
             state_out[at] = fresh
             state_b[at] = fresh.astype(BF16)
 
-    def some_heads(i):
-        for e in range(heads // tokens.groups):
-            one_head(i * (heads // tokens.groups) + e)
-
-    tokens.round(0, some_heads)
-
-    swap.wait()
-
     blocks = span // 16
 
     def scale_rows(i):
-        at = pl.ds(pl.multiple_of(i * 16, 16), 16)
+        at = pl.ds(i * 16, 16)
         for side in range(2):
             weights[side, at] = (weights[side, at].astype(F32) * gain[...]).astype(BF16)
 
-    for k in range(1, tokens.hops):
-        ring.step(k)
-        tokens.round(k, scale_rows if k < tokens.hops - 1 else None)
-        if k == 1:
-            scale_rows = lambda i, first=scale_rows: pl.when(i + 4 < blocks)(lambda: first(i + 4))
-    ring.step(tokens.hops)
+    def first_scale():
+        swap.wait()
+        gain[...] = gain_v[...].astype(F32).reshape(1, width)
+        scale_rows(0)
+
+    one_head(0)
+    one_head(1)
+    work = [functools.partial(one_head, h) for h in range(2, heads)]
+    work += [first_scale] + [functools.partial(scale_rows, i) for i in range(1, blocks)]
+    work = iter(work)
+
+    def beside():
+        piece = next(work, None)
+        if piece is not None:
+            piece()
+
+    for w in range(tokens.waves()):
+        tokens.wave(w, beside)
+        if 1 <= w <= tokens.hops:
+            ring.step(w)
     tokens.last_arrivals()
 
-    depth = tok_v.shape[1]
-    width = nz * ny * depth
     for p in range(2):
         total = jnp.zeros((2 * span, seqs), F32)
         squares = jnp.zeros((1, seqs), F32)
@@ -769,17 +780,12 @@
             (((1,), (1,)), ((), ())),
             preferred_element_type=F32,
         )
-        blank = jnp.zeros_like(product)
-        lanes = jnp.where(
-            (second[p][0] & 1) == 0,
-            jnp.concatenate([product, blank], axis=1),
-            jnp.concatenate([blank, product], axis=1),
-        ).astype(BF16)
         part = out_cols // 2
         for to in range(second[p][1]):
             for side in range(2):
                 at = to * out_cols + side * part
-                out_c[p, to, side] = lanes[at : at + part]
+                halves = [product[at + e : at + e + part // 2] for e in (0, part // 2)]
+                out_c[p, to, side] = jnp.concatenate(halves, axis=1).astype(BF16)
 
         def c_start(i, p=p, n=n):
             d = far_first(i, n)
@@ -799,15 +805,14 @@
             tokens.loop(
                 0, n, lambda s, p=p, side=side: wait_for(in_c.at[p, side, s], c_got.at[p, side, s])
             )
-        sums = jnp.concatenate(
-            [
-                jnp.concatenate(
-                    [in_c[p, side, 2 * j] + in_c[p, side, 2 * j + 1] for j in range(n // 2)], axis=1
+        sums = []
+        for side in range(2):
+            pairs = [[in_c[p, side, 2 * j + e].astype(F32) for e in range(2)] for j in range(n // 2)]
+            for cut_at in (slice(0, 64), slice(64, 128)):
+                sums.append(
+                    jnp.concatenate([each[:, cut_at] for pair in pairs for each in pair], axis=1)
                 )
-                for side in range(2)
-            ],
-            axis=0,
-        )
+        sums = jnp.concatenate(sums, axis=0).astype(BF16)
         moved = jnp.dot(sums, order[p], preferred_element_type=F32)
         result += moved[: out_cols // 2] + moved[out_cols // 2 :]
     result = result.astype(BF16)
@@ -903,7 +908,7 @@
             jax.ShapeDtypeStruct((2, 4, heads, key_size), BF16),
             jax.ShapeDtypeStruct((2, 4, heads, value_size), BF16),
         ),
-        in_specs=[hbm] * 12 + [vmem] * 2,
+        in_specs=[hbm] * 13 + [vmem],
         out_specs=(vmem,) * 4,
         scratch_shapes=[
             pltpu.VMEM((2, depth, seqs), BF16),
@@ -915,6 +920,8 @@
             pltpu.SMEM((heads,), F32),
             pltpu.SMEM((2,), jnp.int32),
             pltpu.SMEM((2,), jnp.int32),
+            pltpu.VMEM((width,), BF16),
+            pltpu.VMEM((1, width), F32),
             pltpu.VMEM((2, 2, 4 * heads, key_size), F32),
             pltpu.VMEM((2 * heads, key_size, value_size), BF16),
             pltpu.VMEM((2, nz, ny, depth, seqs), BF16),
@@ -928,9 +935,9 @@
             pltpu.VMEM((value_size // 128, count, 128), F32),
             pltpu.VMEM((2, 8, cut), BF16),
             pltpu.VMEM((2, nz, 8, cut), BF16),
-            pltpu.VMEM((2, nz, 2, out_cols // 2, 128), BF16),
-            pltpu.VMEM((2, 2, nz, out_cols // 2, 128), BF16),
-            dma((22,)),
+            pltpu.VMEM((2, nz, 2, out_cols // 4, 128), BF16),
+            pltpu.VMEM((2, 2, nz, out_cols // 4, 128), BF16),
+            dma((23,)),
             dma((2, nz, ny)),
             dma((2, max(nz, ny), TorusGather.groups)),
             dma((2, max(nz, ny))),
@@ -970,9 +977,9 @@
                 decay_rate,
                 accepted,
                 lengths,
+                norm_gain,
             ),
         ),
-        norm_gain.astype(F32)[None, :],
         frequency,
     )
     retained, state, new_keys, new_values = put_out(retained, state, new_keys, new_values)

time: 69.2 us -> 76.1 us (1.100)
  Pallas kernels: 67.6 us -> 75.3 us
    pallas_call x1, Pallas kernels: 66.2 us -> 73.9 us  [shards(): pl.pallas_call(functools.partial(kernel, nx, nz, ny), out_shape=(jax.Shap...]
where the time goes in v5:
time: 76.1 us; the launch traced here: 76 us
  Pallas kernels  75.3 us (99%)
    pallas_call x1, Pallas kernels, shards(): pl.pallas_call(functools.partial(kernel, nx, nz, ny), out_shape=(jax.Shap...  73.9 us

profile of v5, /device:TPU:1, one launch (start us, length us, event | category | flops | bytes accessed | tf_op | source)
XLA Modules:
  0.0 76.0 jit_solution(14301732742152358596)
XLA Ops:
  0.6 0.1 maximum_bitcast_fusion.frequency
  0.7 73.9 %shard_map.156 = (bf16[4,32,128]{2,1,0:T(8,128)(2,1)S(1)}, f32[16,128,256]{2,1,0:T(8,128)S(1)}, bf16[2,4,8,128]{3,2,1,0:T(8,128)(2,1)S(1)}, bf16[2,4,8,256]{3,2,1,0:T(8,128)(2,1)S(1)}) custom-call(bf16[4,64,128]{2,1,0:T(8,128)(2,1)} %bitcast.19, bf16[16,4096]{1,0:T(8,128)(2,1)} %bitcast.17, bf16[16,4096]{1,0:T(8,128)(2,1)} %bitcast.18, ...), custom_call_target="tpu_custom_call" | custom-call | tf_op jit(solution)/shard_map/pallas_call | solution.py:903
  74.6 1.4 %shard_map.157 = (bf16[4,32,128]{2,1,0:T(8,128)(2,1)}, f32[16,128,256]{2,1,0:T(8,128)}, bf16[2,4,8,128]{3,2,1,0:T(8,128)(2,1)}, bf16[2,4,8,256]{3,2,1,0:T(8,128)(2,1)}) custom-call(bf16[4,32,128]{2,1,0:T(8,128)(2,1)S(1)} %get-tuple-element.12.refs_0_, f32[16,128,256]{2,1,0:T(8,128)S(1)} %get-tuple-element.13.refs_1_, ...), custom_call_target="tpu_custom_call" | custom-call | tf_op jit(solution)/shard_map/pallas_call | solution.py:860
  (1 shorter events, 0.0 us)

commit v6 on v5

--- a/solution.py
+++ b/solution.py
@@ -138,16 +138,11 @@
             return (1, -1)
         return (1,) if i < self.groups // 2 else (-1,)
 
-    def wave(self, w, beside=None):
-        for k in reversed(range(self.hops)):
-            i = w - k
-            if 0 <= i < self.groups:
-                self.pass_on(k, i, self.ways(k, i))
-                if beside is not None:
-                    beside()
-
-    def waves(self):
-        return self.hops + self.groups - 1
+    def round(self, k, beside=None):
+        for i in range(self.groups):
+            self.pass_on(k, i, self.ways(k, i))
+            if beside is not None:
+                beside()
 
     def last_arrivals(self):
         for i in range(self.groups):
@@ -518,10 +513,11 @@
         if piece is not None:
             piece()
 
-    for w in range(tokens.waves()):
-        tokens.wave(w, beside)
-        if 1 <= w <= tokens.hops:
-            ring.step(w)
+    for k in range(tokens.hops):
+        if k > 0:
+            ring.step(k)
+        tokens.round(k, beside)
+    ring.step(tokens.hops)
     tokens.last_arrivals()
 
     for p in range(2):

time: 76.1 us -> 68.4 us (0.90)
  Pallas kernels: 75.3 us -> 67.5 us
    pallas_call x1, Pallas kernels: 73.9 us -> 66.2 us  [shards(): pl.pallas_call(functools.partial(kernel, nx, nz, ny), out_shape=(jax.Shap...]
where the time goes in v6:
time: 68.4 us; the launch traced here: 68.3 us
  Pallas kernels  67.5 us (99%)
    pallas_call x1, Pallas kernels, shards(): pl.pallas_call(functools.partial(kernel, nx, nz, ny), out_shape=(jax.Shap...  66.2 us
    pallas_call x1, Pallas kernels, put_out(): pl.pallas_call(put_kernel, out_shape=tuple((jax.ShapeDtypeStruct(v.shape,...  1.37 us

profile of v6, /device:TPU:1, one launch (start us, length us, event | category | flops | bytes accessed | tf_op | source)
XLA Modules:
  0.0 68.3 jit_solution(137614043656032875)
XLA Ops:
  0.6 0.1 maximum_bitcast_fusion.frequency
  0.7 66.2 %shard_map.156 = (bf16[4,32,128]{2,1,0:T(8,128)(2,1)S(1)}, f32[16,128,256]{2,1,0:T(8,128)S(1)}, bf16[2,4,8,128]{3,2,1,0:T(8,128)(2,1)S(1)}, bf16[2,4,8,256]{3,2,1,0:T(8,128)(2,1)S(1)}) custom-call(bf16[4,64,128]{2,1,0:T(8,128)(2,1)} %bitcast.19, bf16[16,4096]{1,0:T(8,128)(2,1)} %bitcast.17, bf16[16,4096]{1,0:T(8,128)(2,1)} %bitcast.18, ...), custom_call_target="tpu_custom_call" | custom-call | tf_op jit(solution)/shard_map/pallas_call | solution.py:899
  66.9 1.4 %shard_map.157 = (bf16[4,32,128]{2,1,0:T(8,128)(2,1)}, f32[16,128,256]{2,1,0:T(8,128)}, bf16[2,4,8,128]{3,2,1,0:T(8,128)(2,1)}, bf16[2,4,8,256]{3,2,1,0:T(8,128)(2,1)}) custom-call(bf16[4,32,128]{2,1,0:T(8,128)(2,1)S(1)} %get-tuple-element.12.refs_0_, f32[16,128,256]{2,1,0:T(8,128)S(1)} %get-tuple-element.13.refs_1_, ...), custom_call_target="tpu_custom_call" | custom-call | tf_op jit(solution)/shard_map/pallas_call | solution.py:856
  (1 shorter events, 0.0 us)

commit v7 on v6

--- a/solution.py
+++ b/solution.py
@@ -32,8 +32,8 @@
 
 
 class TorusGather:
-    groups = 4
-    turn = (0, 1, 3, 2)
+    groups = 8
+    turn = (0, 1, 7, 2, 6, 3, 5, 4)
 
     def __init__(self, own, held, arrived, ring_arrived, first_sent, ring_sent, nz, ny):
         self.own, self.held, self.arrived, self.ring_arrived = own, held, arrived, ring_arrived
@@ -87,16 +87,16 @@
     def group_at(self, p, q, s):
         return self.at(self.held, p, pl.ds(q * self.size, self.size), s)
 
-    def ring_copy(self, p, k, i, way):
+    def ring_copy(self, p, k, i, way, reach=1):
         s, n, axis = self.second[p]
         q, origin = self.group(p, i), wrap(s - way * k + n, n)
         block = self.group_at(p, q, origin)
         return self.copy(
             block,
             block,
-            self.ring_sent.at[p, (1 + way) // 2, k, i],
+            self.ring_sent.at[p, (1 + way) // 2, k + reach - 1, i],
             self.ring_arrived.at[p, origin, q],
-            {axis: wrap(s + way + n, n)},
+            {axis: wrap(s + reach * way + n, n)},
         )
 
     def wait_chunk(self, p, f, s):
@@ -123,6 +123,8 @@
             else:
                 for way in (1, -1):
                     self.wait_group(p, i, wrap(s - way * k + n, n))
+                    if k == self.hops - 2 and way == self.far_way(i):
+                        self.ring_copy(p, k, i, way, 2).start()
                     if way in ways:
                         self.ring_copy(p, k, i, way).start()
 
@@ -134,9 +136,10 @@
         lax.fori_loop(low, high, body, 0)
 
     def ways(self, k, i):
-        if k < self.hops - 1:
-            return (1, -1)
-        return (1,) if i < self.groups // 2 else (-1,)
+        return (1, -1) if k < self.hops - 1 else ()
+
+    def far_way(self, i):
+        return 1 if i % 2 else -1
 
     def round(self, k, beside=None):
         for i in range(self.groups):
@@ -161,6 +164,8 @@
                 for p in range(2):
                     for way in self.ways(k, i):
                         self.ring_copy(p, k, i, way).wait_send()
+                    if k == self.hops - 2:
+                        self.ring_copy(p, k, i, self.far_way(i), 2).wait_send()
 
 
 class WeightRing:
@@ -188,14 +193,14 @@
             device_id_type=MESH,
         )
 
-    def ring_copy(self, p, k, way):
+    def ring_copy(self, p, k, way, reach=1):
         s, n, axis = self.second[p]
         origin = wrap(s - way * k + n, n)
         return self.copy(
             self.block(p, origin, self.x),
-            self.sent.at[p, (1 + way) // 2, k],
+            self.sent.at[p, (1 + way) // 2, k + reach - 1],
             self.arrived.at[p, origin],
-            {axis: wrap(s + way + n, n)},
+            {axis: wrap(s + reach * way + n, n)},
         )
 
     def side_copy(self, p, origin, way):
@@ -222,9 +227,7 @@
         )
 
     def forward_ways(self, p, k):
-        if k < self.hops - 1:
-            return (1, -1)
-        return (self.on_way(p),) if k == self.hops - 1 else ()
+        return (1, -1) if k < self.hops - 1 else ()
 
     def step(self, k):
         for p in range(2):
@@ -242,6 +245,8 @@
                 for to in ways if k == 0 else (way,):
                     if to in ways:
                         self.ring_copy(p, k, to).start()
+                        if k == self.hops - 2 and to == self.on_way(p):
+                            self.ring_copy(p, k, to, 2).start()
                 for to in (1, -1):
                     self.side_copy(p, origin, to).start()
 
@@ -274,6 +279,7 @@
             for k in range(self.hops):
                 for way in self.forward_ways(p, k):
                     self.ring_copy(p, k, way).wait_send()
+            self.ring_copy(p, self.hops - 2, self.on_way(p), 2).wait_send()
 
             def done(origin, _, p=p):
                 for way in (1, -1):

time: 68.4 us -> 68.3 us (level)
  no operation moved by 1% of the time
where the time goes in v7:
time: 68.3 us; the launch traced here: 68.2 us
  Pallas kernels  67.4 us (99%)
    pallas_call x1, Pallas kernels, shards(): pl.pallas_call(functools.partial(kernel, nx, nz, ny), out_shape=(jax.Shap...  66.1 us
    pallas_call x1, Pallas kernels, put_out(): pl.pallas_call(put_kernel, out_shape=tuple((jax.ShapeDtypeStruct(v.shape,...  1.37 us

profile of v7, /device:TPU:1, one launch (start us, length us, event | category | flops | bytes accessed | tf_op | source)
XLA Modules:
  0.0 68.2 jit_solution(2015056070371250605)
XLA Ops:
  0.6 0.1 maximum_bitcast_fusion.frequency
  0.7 66.1 %shard_map.156 = (bf16[4,32,128]{2,1,0:T(8,128)(2,1)S(1)}, f32[16,128,256]{2,1,0:T(8,128)S(1)}, bf16[2,4,8,128]{3,2,1,0:T(8,128)(2,1)S(1)}, bf16[2,4,8,256]{3,2,1,0:T(8,128)(2,1)S(1)}) custom-call(bf16[4,64,128]{2,1,0:T(8,128)(2,1)} %bitcast.19, bf16[16,4096]{1,0:T(8,128)(2,1)} %bitcast.17, bf16[16,4096]{1,0:T(8,128)(2,1)} %bitcast.18, ...), custom_call_target="tpu_custom_call" | custom-call | tf_op jit(solution)/shard_map/pallas_call | solution.py:905
  66.8 1.4 %shard_map.157 = (bf16[4,32,128]{2,1,0:T(8,128)(2,1)}, f32[16,128,256]{2,1,0:T(8,128)}, bf16[2,4,8,128]{3,2,1,0:T(8,128)(2,1)}, bf16[2,4,8,256]{3,2,1,0:T(8,128)(2,1)}) custom-call(bf16[4,32,128]{2,1,0:T(8,128)(2,1)S(1)} %get-tuple-element.12.refs_0_, f32[16,128,256]{2,1,0:T(8,128)S(1)} %get-tuple-element.13.refs_1_, ...), custom_call_target="tpu_custom_call" | custom-call | tf_op jit(solution)/shard_map/pallas_call | solution.py:862
  (1 shorter events, 0.0 us)

commit v8 on v7

--- a/solution.py
+++ b/solution.py
@@ -141,11 +141,10 @@
     def far_way(self, i):
         return 1 if i % 2 else -1
 
-    def round(self, k, beside=None):
-        for i in range(self.groups):
-            self.pass_on(k, i, self.ways(k, i))
-            if beside is not None:
-                beside()
+    def steps(self):
+        lag = self.groups // 2
+        every = [(k, i) for k in range(self.hops) for i in range(self.groups)]
+        return sorted(every, key=lambda at: (at[1] + lag * at[0], at[0]))
 
     def last_arrivals(self):
         for i in range(self.groups):
@@ -519,10 +518,11 @@
         if piece is not None:
             piece()
 
-    for k in range(tokens.hops):
-        if k > 0:
+    for k, i in tokens.steps():
+        if k > 0 and i == 0:
             ring.step(k)
-        tokens.round(k, beside)
+        tokens.pass_on(k, i, tokens.ways(k, i))
+        beside()
     ring.step(tokens.hops)
     tokens.last_arrivals()
 

time: 68.3 us -> 70.1 us (1.026)
  Pallas kernels: 67.4 us -> 69.2 us
    pallas_call x1, Pallas kernels: 66.1 us -> 67.9 us  [shards(): pl.pallas_call(functools.partial(kernel, nx, nz, ny), out_shape=(jax.Shap...]
where the time goes in v8:
time: 70.1 us; the launch traced here: 70 us
  Pallas kernels  69.2 us (99%)
    pallas_call x1, Pallas kernels, shards(): pl.pallas_call(functools.partial(kernel, nx, nz, ny), out_shape=(jax.Shap...  67.9 us

profile of v8, /device:TPU:1, one launch (start us, length us, event | category | flops | bytes accessed | tf_op | source)
XLA Modules:
  0.0 70.0 jit_solution(7136372845150743015)
XLA Ops:
  0.6 0.1 maximum_bitcast_fusion.frequency
  0.7 67.9 %shard_map.156 = (bf16[4,32,128]{2,1,0:T(8,128)(2,1)S(1)}, f32[16,128,256]{2,1,0:T(8,128)S(1)}, bf16[2,4,8,128]{3,2,1,0:T(8,128)(2,1)S(1)}, bf16[2,4,8,256]{3,2,1,0:T(8,128)(2,1)S(1)}) custom-call(bf16[4,64,128]{2,1,0:T(8,128)(2,1)} %bitcast.19, bf16[16,4096]{1,0:T(8,128)(2,1)} %bitcast.17, bf16[16,4096]{1,0:T(8,128)(2,1)} %bitcast.18, ...), custom_call_target="tpu_custom_call" | custom-call | tf_op jit(solution)/shard_map/pallas_call | solution.py:905
  68.6 1.4 %shard_map.157 = (bf16[4,32,128]{2,1,0:T(8,128)(2,1)}, f32[16,128,256]{2,1,0:T(8,128)}, bf16[2,4,8,128]{3,2,1,0:T(8,128)(2,1)}, bf16[2,4,8,256]{3,2,1,0:T(8,128)(2,1)}) custom-call(bf16[4,32,128]{2,1,0:T(8,128)(2,1)S(1)} %get-tuple-element.12.refs_0_, f32[16,128,256]{2,1,0:T(8,128)S(1)} %get-tuple-element.13.refs_1_, ...), custom_call_target="tpu_custom_call" | custom-call | tf_op jit(solution)/shard_map/pallas_call | solution.py:862
  (1 shorter events, 0.0 us)

commit v9 on v7

--- a/solution.py
+++ b/solution.py
@@ -520,11 +520,21 @@
             piece()
 
     for k in range(tokens.hops):
+        tokens.round(k, beside)
         if k > 0:
             ring.step(k)
-        tokens.round(k, beside)
-    ring.step(tokens.hops)
     tokens.last_arrivals()
+
+    def a_copy(p, d):
+        to = wrap(z + d, nz)
+        return pltpu.make_async_remote_copy(
+            src_ref=out_a.at[p, to],
+            dst_ref=in_a.at[p, z],
+            send_sem=a_sent.at[p, d],
+            recv_sem=a_got.at[p, z],
+            device_id={"kv_0": to},
+            device_id_type=MESH,
+        )
 
     for p in range(2):
         total = jnp.zeros((2 * span, seqs), F32)
@@ -544,34 +554,22 @@
             )
             turned = part.T.astype(BF16)
             for to in range(nz):
-                out_a[to, side, p] = turned[2 * ny * to : 2 * ny * (to + 1)]
-
-    def a_copy(d):
-        to = wrap(z + d, nz)
-        return pltpu.make_async_remote_copy(
-            src_ref=out_a.at[to],
-            dst_ref=in_a.at[z],
-            send_sem=a_sent.at[d],
-            recv_sem=a_got.at[z],
-            device_id={"kv_0": to},
-            device_id_type=MESH,
-        )
-
-    def a_wait(d):
-        came = wrap(z + d, nz)
-        pltpu.make_async_remote_copy(
-            src_ref=in_a.at[came],
-            dst_ref=in_a.at[came],
-            send_sem=a_sent.at[0],
-            recv_sem=a_got.at[came],
-            device_id=partner,
-            device_id_type=MESH,
-        ).wait_recv()
-
-    tokens.loop(1, nz, lambda i: a_copy(far_first(i, nz)).start())
-    own_a = pltpu.make_async_copy(out_a.at[z], in_a.at[z], local.at[10])
-    own_a.start()
-    ring.share_on()
+                out_a[p, to, side] = turned[2 * ny * to : 2 * ny * (to + 1)]
+        tokens.loop(1, nz, lambda i, p=p: a_copy(p, far_first(i, nz)).start())
+        pltpu.make_async_copy(out_a.at[p, z], in_a.at[p, z], a_got.at[p, z]).start()
+
+    def a_wait(came):
+        for p in range(2):
+            pltpu.make_async_remote_copy(
+                src_ref=in_a.at[p, came],
+                dst_ref=in_a.at[p, came],
+                send_sem=a_sent.at[0, 0],
+                recv_sem=a_got.at[p, came],
+                device_id=partner,
+                device_id_type=MESH,
+            ).wait_recv()
+
+    ring.step(tokens.hops)
 
     shift = heads.bit_length() - 1
 
@@ -598,16 +596,15 @@
         0.0,
     )
 
-    own_a.wait()
-    tokens.loop(1, nz, a_wait)
+    tokens.loop(0, nz, a_wait)
 
     mid[...] = in_a[...].reshape(nz * 4 * 2 * ny, 128).astype(F32)
-    stride = 4 * 2 * ny
+    stride = 2 * 2 * ny
     for to in range(ny):
         for side in range(2):
             for s in range(2):
                 parts = [
-                    mid[pl.ds(side * 4 * ny + p * 2 * ny + 2 * to + s, nz, stride=stride), :]
+                    mid[pl.ds(p * nz * stride + side * 2 * ny + 2 * to + s, nz, stride=stride), :]
                     for p in range(2)
                 ]
                 out_b[to, side, s] = jnp.concatenate(parts, axis=0).astype(BF16)
@@ -645,6 +642,7 @@
     b_copy(0, False).start()
     own_b = pltpu.make_async_copy(out_b.at[y, tp], in_b.at[y, tp], local.at[11])
     own_b.start()
+    ring.share_on()
 
     lane = iota((128, 2 * key_size + 2 * value_size), 0)
     column = iota((128, 2 * key_size + 2 * value_size), 1)
@@ -766,7 +764,7 @@
         pltpu.make_async_remote_copy(
             src_ref=block,
             dst_ref=block,
-            send_sem=a_sent.at[0],
+            send_sem=a_sent.at[0, 0],
             recv_sem=arrived,
             device_id=partner,
             device_id_type=MESH,
@@ -832,7 +830,8 @@
     tokens.loop(1, ny, late_done)
     for p in range(2):
         c_copy(p, 0, False).wait_send()
-    tokens.loop(1, nz, lambda d: a_copy(d).wait_send())
+    for p in range(2):
+        tokens.loop(1, nz, lambda d, p=p: a_copy(p, d).wait_send())
 
     def b_done(d):
         b_copy(d, True).wait_send()
@@ -929,8 +928,8 @@
             pltpu.VMEM((2, nz, ny, depth, seqs), BF16),
             pltpu.VMEM((128 * ny, 2 * key_size + 2 * value_size), BF16),
             pltpu.VMEM((2, 4 * seqs, 4 * seqs), BF16),
-            pltpu.VMEM((nz, 2, 2, 2 * ny, 128), BF16),
-            pltpu.VMEM((nz, 2, 2, 2 * ny, 128), BF16),
+            pltpu.VMEM((2, nz, 2, 2 * ny, 128), BF16),
+            pltpu.VMEM((2, nz, 2, 2 * ny, 128), BF16),
             pltpu.VMEM((nz * 8 * ny, 128), F32),
             pltpu.VMEM((ny, 2, 2, 2 * nz, 128), BF16),
             pltpu.VMEM((ny, 2, 2, 2 * nz, 128), BF16),
@@ -955,8 +954,8 @@
             dma((2, nz, 2)),
             dma((2, 2, nz)),
             dma((4,)),
-            dma((nz,)),
-            dma((nz,)),
+            dma((2, nz)),
+            dma((2, nz)),
             dma((ny, 2)),
             dma((ny, 2)),
         ],

time: 68.3 us -> 68.1 us (level)
  no operation moved by 1% of the time
where the time goes in v9:
time: 68.1 us; the launch traced here: 68 us
  Pallas kernels  67.3 us (99%)
    pallas_call x1, Pallas kernels, shards(): pl.pallas_call(functools.partial(kernel, nx, nz, ny), out_shape=(jax.Shap...  65.9 us
    pallas_call x1, Pallas kernels, put_out(): pl.pallas_call(put_kernel, out_shape=tuple((jax.ShapeDtypeStruct(v.shape,...  1.37 us

profile of v9, /device:TPU:1, one launch (start us, length us, event | category | flops | bytes accessed | tf_op | source)
XLA Modules:
  0.0 68.0 jit_solution(6191683266966539385)
XLA Ops:
  0.6 0.1 maximum_bitcast_fusion.frequency
  0.7 65.9 %shard_map.156 = (bf16[4,32,128]{2,1,0:T(8,128)(2,1)S(1)}, f32[16,128,256]{2,1,0:T(8,128)S(1)}, bf16[2,4,8,128]{3,2,1,0:T(8,128)(2,1)S(1)}, bf16[2,4,8,256]{3,2,1,0:T(8,128)(2,1)S(1)}) custom-call(bf16[4,64,128]{2,1,0:T(8,128)(2,1)} %bitcast.19, bf16[16,4096]{1,0:T(8,128)(2,1)} %bitcast.17, bf16[16,4096]{1,0:T(8,128)(2,1)} %bitcast.18, ...), custom_call_target="tpu_custom_call" | custom-call | tf_op jit(solution)/shard_map/pallas_call | solution.py:904
  66.6 1.4 %shard_map.157 = (bf16[4,32,128]{2,1,0:T(8,128)(2,1)}, f32[16,128,256]{2,1,0:T(8,128)}, bf16[2,4,8,128]{3,2,1,0:T(8,128)(2,1)}, bf16[2,4,8,256]{3,2,1,0:T(8,128)(2,1)}) custom-call(bf16[4,32,128]{2,1,0:T(8,128)(2,1)S(1)} %get-tuple-element.12.refs_0_, f32[16,128,256]{2,1,0:T(8,128)S(1)} %get-tuple-element.13.refs_1_, ...), custom_call_target="tpu_custom_call" | custom-call | tf_op jit(solution)/shard_map/pallas_call | solution.py:861
  (1 shorter events, 0.0 us)

commit v10 on v9

--- a/solution.py
+++ b/solution.py
@@ -570,6 +570,7 @@
             ).wait_recv()
 
     ring.step(tokens.hops)
+    tokens.finish()
 
     shift = heads.bit_length() - 1
 
@@ -746,6 +747,16 @@
             hit = (row_seq == target) & (row_prop == p)
             order[part, :, pl.ds(seqs * p, seqs)] = jnp.where(hit, 1.0, 0.0).astype(BF16)
     ring.all_here()
+    ring.finish()
+    for p in range(2):
+        tokens.loop(1, nz, lambda d, p=p: a_copy(p, d).wait_send())
+
+    def b_done(d):
+        b_copy(d, True).wait_send()
+        b_copy(d, False).wait_send()
+
+    tokens.loop(1, ny, b_done)
+    b_copy(0, False).wait_send()
 
     def c_copy(p, d, same):
         s, n, axis = second[p]
@@ -798,6 +809,12 @@
         pltpu.make_async_copy(
             out_c.at[p, s, tp], in_c.at[p, tp, s], c_got.at[p, tp, s]
         ).start()
+
+    def g_done(d):
+        for p in range(2):
+            g_copy(p, d).wait_send()
+
+    tokens.loop(1, ny, g_done)
     result = jnp.zeros((out_cols // 2, 4 * seqs), F32)
     for p in range(2):
         n = second[p][1]
@@ -818,27 +835,14 @@
     result = result.astype(BF16)
     for p in range(4):
         ret_out[p] = result[:, p * seqs : (p + 1) * seqs]
-    tokens.finish()
-    ring.finish()
-
-    def late_done(d):
+    def c_done(d):
         for p in range(2):
-            g_copy(p, d).wait_send()
             for same in (True, False):
                 c_copy(p, d, same).wait_send()
 
-    tokens.loop(1, ny, late_done)
+    tokens.loop(1, ny, c_done)
     for p in range(2):
         c_copy(p, 0, False).wait_send()
-    for p in range(2):
-        tokens.loop(1, nz, lambda d, p=p: a_copy(p, d).wait_send())
-
-    def b_done(d):
-        b_copy(d, True).wait_send()
-        b_copy(d, False).wait_send()
-
-    tokens.loop(1, ny, b_done)
-    b_copy(0, False).wait_send()
 
 
 def in_hbm(value):

time: 68.1 us -> 67.6 us (level)
  no operation moved by 1% of the time
where the time goes in v10:
time: 67.6 us; the launch traced here: 67.4 us
  Pallas kernels  66.7 us (99%)
    pallas_call x1, Pallas kernels, shards(): pl.pallas_call(functools.partial(kernel, nx, nz, ny), out_shape=(jax.Shap...  65.3 us
    pallas_call x1, Pallas kernels, put_out(): pl.pallas_call(put_kernel, out_shape=tuple((jax.ShapeDtypeStruct(v.shape,...  1.37 us

profile of v10, /device:TPU:1, one launch (start us, length us, event | category | flops | bytes accessed | tf_op | source)
XLA Modules:
  0.0 67.4 jit_solution(9861168581318281151)
XLA Ops:
  0.6 0.1 maximum_bitcast_fusion.frequency
  0.7 65.3 %shard_map.156 = (bf16[4,32,128]{2,1,0:T(8,128)(2,1)S(1)}, f32[16,128,256]{2,1,0:T(8,128)S(1)}, bf16[2,4,8,128]{3,2,1,0:T(8,128)(2,1)S(1)}, bf16[2,4,8,256]{3,2,1,0:T(8,128)(2,1)S(1)}) custom-call(bf16[4,64,128]{2,1,0:T(8,128)(2,1)} %bitcast.19, bf16[16,4096]{1,0:T(8,128)(2,1)} %bitcast.17, bf16[16,4096]{1,0:T(8,128)(2,1)} %bitcast.18, ...), custom_call_target="tpu_custom_call" | custom-call | tf_op jit(solution)/shard_map/pallas_call | solution.py:908
  66.1 1.4 %shard_map.157 = (bf16[4,32,128]{2,1,0:T(8,128)(2,1)}, f32[16,128,256]{2,1,0:T(8,128)}, bf16[2,4,8,128]{3,2,1,0:T(8,128)(2,1)}, bf16[2,4,8,256]{3,2,1,0:T(8,128)(2,1)}) custom-call(bf16[4,32,128]{2,1,0:T(8,128)(2,1)S(1)} %get-tuple-element.12.refs_0_, f32[16,128,256]{2,1,0:T(8,128)S(1)} %get-tuple-element.13.refs_1_, ...), custom_call_target="tpu_custom_call" | custom-call | tf_op jit(solution)/shard_map/pallas_call | solution.py:865
  (1 shorter events, 0.0 us)
